TPU v7x, 128 devices: a whole 4x4x4 slice. The times are simulated.
128 devices in a mesh: ep: 32 (over z, y, core), tp: 4 (over x).
Axes of the slice: x: 4, y: 4, z: 4, core: 2. Of those that a mesh axis runs over, the one named last changes fastest.
Arguments:
- q_latent: bfloat16 [16384, 512], P(('ep', 'tp')), may hold values from -6 to 6
- kv_latent: bfloat16 [16384, 256], P(('ep', 'tp')), may hold values from -6 to 6
- rope_key: bfloat16 [16384, 32], P(('ep', 'tp')), may hold values from -240 to 240
- q_gain: float32 [512], replicated, may hold values from 0.1 to 1.9
- kv_gain: float32 [256], replicated, may hold values from 0.1 to 1.9
- w_query: bfloat16 [512, 1024], P(None, 'tp'), may hold values from -0.25 to 0.25
- w_query_rot: bfloat16 [512, 512], P(None, 'tp'), may hold values from -0.25 to 0.25
- w_key: bfloat16 [256, 1024], P(None, 'tp'), may hold values from -0.375 to 0.375
- w_value: bfloat16 [256, 1024], P(None, 'tp'), may hold values from -0.375 to 0.375
- w_mix_out: bfloat16 [1024, 2048], P('tp'), may hold values from -0.1875 to 0.1875
- expert_input: bfloat16 [16384, 2048], P(('ep', 'tp')), may hold values from -6 to 6
- ffn_gain: float32 [2048], replicated, may hold values from 0.1 to 1.9
- expert_ids: int32 [16384, 4], P(('ep', 'tp')), may hold values from 0 to 31, all different within a row; in each aligned block of 128 rows (0 to 127, 128 to 255, ...) at most 24 rows name the same one
- route_weights: float32 [16384, 4], P(('ep', 'tp')), may hold values from 0.2 to 1
- w_gate_exp: bfloat16 [32, 2048, 1024], P('ep', None, 'tp'), may hold values from -0.125 to 0.125
- w_up_exp: bfloat16 [32, 2048, 1024], P('ep', None, 'tp'), may hold values from -0.125 to 0.125
- w_down_exp: bfloat16 [32, 1024, 2048], P('ep', 'tp'), may hold values from -0.1875 to 0.1875
Outputs:
- mixer_out: bfloat16 [16384, 2048], P(('ep', 'tp'))
- expert_out: bfloat16 [16384, 2048], P(('ep', 'tp'))
Inputs may be any that keep to these rules, and one draw needn't show every extreme that they name: `expert_ids`: the experts of a row are all different. In the rows of one device (aligned blocks of 128 tokens) no expert is named by more than 24 rows, a bound that some block reaches.
All inputs are finite; a program needn't handle non-finite values.
Results may differ from a plain program's by a relative error of at most 0.012.
The roundings to bfloat16 on the way count: a program that leaves them out, or rounds other values in their place, can miss the bound.
Values may be sent and summed in bfloat16 or wider, within the bound.
No kernel may reach another device: no remote copies, remote signals or barrier semaphores. Data moves between devices by JAX's collectives and lax.ppermute only.
A program may use at most 128 MiB of HBM per device.

v0:
```python
import jax
import jax.numpy as jnp
from jax import lax
from jax.sharding import PartitionSpec as P

D = 2048
NOPE = 64
ROPE = 32
VD = 64
TOPK = 4
SEG = 64


norm_epsilon = 1e-06
rope_base = 10000.0
masked_score = -1e30


def rms_scale(values_in, gain_vec):
    floats = values_in.astype(jnp.float32)
    return (
        floats
        * lax.rsqrt(jnp.mean(floats * floats, axis=-1, keepdims=True) + norm_epsilon)
        * gain_vec
    )


def tables(positions):
    half_width = ROPE // 2
    frequency = rope_base ** (-jnp.arange(half_width, dtype=jnp.float32) / half_width)
    angles = positions.astype(jnp.float32)[:, None] * frequency[None, :]
    return (jnp.cos(angles), jnp.sin(angles))


def rotate_pairs(values_in, cosine, sine_table):
    half_width = values_in.shape[-1] // 2
    first, second = (values_in[..., :half_width], values_in[..., half_width:])
    return jnp.concatenate(
        [first * cosine - second * sine_table, first * sine_table + second * cosine], axis=-1
    )


def on_device(
    q_latent,
    kv_latent,
    rope_key,
    q_gain,
    kv_gain,
    w_query,
    w_query_rot,
    w_key,
    w_value,
    w_mix_out,
    expert_input,
    ffn_gain,
    expert_ids,
    route_weights,
    w_gate_exp,
    w_up_exp,
    w_down_exp,
):
    tok_rows = q_latent.shape[0]
    tp_count = lax.axis_size("tp")
    group_rows = tp_count * tok_rows
    group_start = lax.axis_index("ep") * group_rows
    heads_here = w_key.shape[1] // NOPE
    score_scale = (NOPE + ROPE) ** (-0.5)
    shard_rows = lax.all_gather(q_latent, "tp", axis=0, tiled=True)
    row_count = shard_rows.shape[0]
    positions = group_start + jnp.arange(row_count, dtype=jnp.int32)
    cosine, sine_table = tables(positions)
    normed = rms_scale(shard_rows, q_gain).astype(jnp.bfloat16)
    plain = jnp.dot(normed, w_query, preferred_element_type=jnp.float32).astype(jnp.bfloat16)
    turned = jnp.dot(normed, w_query_rot, preferred_element_type=jnp.float32).reshape(
        row_count, heads_here, ROPE
    )
    turned = rotate_pairs(turned, cosine[:, None, :], sine_table[:, None, :]).astype(jnp.bfloat16)
    queries = jnp.concatenate([plain, turned.reshape(row_count, heads_here * ROPE)], axis=1)
    q_plain = queries[:, : heads_here * NOPE].reshape(group_rows, heads_here, NOPE)
    q_turned = queries[:, heads_here * NOPE :].reshape(group_rows, heads_here, ROPE)
    query_segment = (group_start + jnp.arange(group_rows, dtype=jnp.int32)) // SEG
    last_segment = (group_start + group_rows - 1) // SEG
    start_state = (
        jnp.full((heads_here, group_rows), masked_score, jnp.float32),
        jnp.zeros((heads_here, group_rows), jnp.float32),
        jnp.zeros((heads_here, group_rows, VD), jnp.float32),
    )
    first_row = jnp.int32(0)
    latents = lax.all_gather(kv_latent, ("ep", "tp"), axis=0, tiled=True)
    rope_rows = lax.all_gather(rope_key, ("ep", "tp"), axis=0, tiled=True)
    shard_count = latents.shape[0] // tok_rows
    grouping = 1
    for divisor in range(1, shard_count + 1):
        if shard_count % divisor == 0 and divisor * tok_rows <= max(512, tok_rows):
            grouping = divisor
    key_rows = grouping * tok_rows

    def key_work(state, offset):
        run_max, weight_sum, weighted = state
        latent_block = lax.dynamic_slice_in_dim(latents, offset, key_rows, 0)
        rope_block = lax.dynamic_slice_in_dim(rope_rows, offset, key_rows, 0)
        positions = first_row + offset + jnp.arange(key_rows, dtype=jnp.int32)
        cosine, sine_table = tables(positions)
        normed = rms_scale(latent_block, kv_gain).astype(jnp.bfloat16)
        k_plain = jnp.dot(normed, w_key, preferred_element_type=jnp.float32).astype(jnp.bfloat16)
        k_plain = k_plain.reshape(key_rows, heads_here, NOPE)
        values = jnp.dot(normed, w_value, preferred_element_type=jnp.float32).astype(jnp.bfloat16)
        values = values.reshape(key_rows, heads_here, VD)
        k_turned = rotate_pairs(rope_block.astype(jnp.float32), cosine, sine_table).astype(
            jnp.bfloat16
        )
        scores = jnp.einsum("qhd,khd->hqk", q_plain, k_plain, preferred_element_type=jnp.float32)
        scores = scores + jnp.einsum(
            "qhd,kd->hqk", q_turned, k_turned, preferred_element_type=jnp.float32
        )
        scores = scores * score_scale
        allowed = (positions // SEG)[None, :] <= query_segment[:, None]
        scores = jnp.where(allowed[None], scores, masked_score)
        new_max = jnp.maximum(run_max, jnp.max(scores, axis=-1))
        weights = jnp.where(allowed[None], jnp.exp(scores - new_max[:, :, None]), 0.0)
        factor = jnp.exp(run_max - new_max)
        weight_sum = weight_sum * factor + jnp.sum(weights, axis=-1)
        weighted = weighted * factor[:, :, None] + jnp.einsum(
            "hqk,khd->hqd", weights.astype(jnp.bfloat16), values, preferred_element_type=jnp.float32
        )
        return (new_max, weight_sum, weighted)

    def key_step(state, block_number):
        offset = block_number * key_rows
        visible = (first_row + offset) // SEG <= last_segment
        updated = lax.cond(
            visible, lambda carried: key_work(carried, offset), lambda carried: carried, state
        )
        return (updated, None)

    result_state, _ = lax.scan(
        key_step, start_state, jnp.arange(shard_count // grouping, dtype=jnp.int32)
    )
    run_max, weight_sum, weighted = result_state
    attention = (
        (weighted / weight_sum[:, :, None])
        .transpose(1, 0, 2)
        .astype(jnp.bfloat16)
        .reshape(group_rows, heads_here * VD)
    )
    chosen = attention
    partial_out = jnp.dot(chosen, w_mix_out, preferred_element_type=jnp.float32).astype(
        jnp.bfloat16
    )
    mixer_out = lax.psum_scatter(
        lax.optimization_barrier(partial_out).astype(jnp.float32).astype(jnp.bfloat16),
        "tp",
        scatter_dimension=0,
        tiled=True,
    )
    expert_count = lax.axis_size("ep")
    slot_count = 3 * tok_rows * TOPK // (2 * expert_count)
    gate_weight = w_gate_exp[0]
    up_weight = w_up_exp[0]
    down_weight = w_down_exp[0]
    normed = rms_scale(expert_input, ffn_gain).astype(jnp.bfloat16)
    routed = expert_ids.reshape(-1)
    onehot = (routed[:, None] == jnp.arange(expert_count, dtype=jnp.int32)[None, :]).astype(
        jnp.int32
    )
    slot_number = jnp.sum((jnp.cumsum(onehot, axis=0) - 1) * onehot, axis=-1)
    slot_place = (routed * slot_count + slot_number).reshape(tok_rows, TOPK)
    slot_line = jnp.arange(expert_count * slot_count, dtype=jnp.int32)
    picks = [
        (slot_place[:, route_rank][:, None] == slot_line[None, :]).astype(jnp.bfloat16)
        for route_rank in range(TOPK)
    ]
    dispatch = picks[0]
    for route_rank in range(1, TOPK):
        dispatch = dispatch + picks[route_rank]
    outgoing = lax.dot_general(
        dispatch, normed, (((0,), (0,)), ((), ())), preferred_element_type=jnp.float32
    ).astype(jnp.bfloat16)
    copies = jnp.broadcast_to(
        outgoing.reshape(expert_count, 1, slot_count, D), (expert_count, tp_count, slot_count, D)
    )
    copies = copies.reshape(expert_count * tp_count, slot_count, D)
    arrived = lax.all_to_all(copies, ("ep", "tp"), split_axis=0, concat_axis=0, tiled=True)
    sources, item_count, feature_width = arrived.shape
    chosen = arrived.reshape(sources * item_count, feature_width)
    gate_part = jnp.dot(chosen, gate_weight, preferred_element_type=jnp.float32)
    up_part = jnp.dot(chosen, up_weight, preferred_element_type=jnp.float32)
    hidden = (jax.nn.silu(gate_part) * up_part).astype(jnp.bfloat16)
    partial_out = jnp.dot(hidden, down_weight, preferred_element_type=jnp.float32).astype(
        jnp.bfloat16
    )
    returned = lax.all_to_all(
        partial_out.reshape(sources, item_count, feature_width),
        ("ep", "tp"),
        split_axis=0,
        concat_axis=0,
        tiled=True,
    )
    block_parts = returned.reshape(expert_count, tp_count, slot_count, D).astype(jnp.float32)
    results = (
        jnp.sum(block_parts, axis=1).astype(jnp.bfloat16).reshape(expert_count * slot_count, D)
    )
    combined = jnp.zeros((tok_rows, D), jnp.float32)
    for route_rank in range(TOPK):
        fetched = jnp.dot(picks[route_rank], results, preferred_element_type=jnp.float32)
        combined = combined + route_weights[:, route_rank : route_rank + 1] * fetched
    expert_out = combined.astype(jnp.bfloat16)
    return (mixer_out, expert_out)


def solution(mesh):
    return jax.shard_map(
        on_device,
        mesh=mesh,
        in_specs=(
            P(("ep", "tp"), None),
            P(("ep", "tp"), None),
            P(("ep", "tp"), None),
            P(),
            P(),
            P(None, "tp"),
            P(None, "tp"),
            P(None, "tp"),
            P(None, "tp"),
            P("tp", None),
            P(("ep", "tp"), None),
            P(),
            P(("ep", "tp"), None),
            P(("ep", "tp"), None),
            P("ep", None, "tp"),
            P("ep", None, "tp"),
            P("ep", "tp", None),
        ),
        out_specs=(P(("ep", "tp"), None), P(("ep", "tp"), None)),
        check_vma=False,
    )
```

profile of v0, /device:TPU:1, one launch (start us, length us, event | category | flops | bytes accessed | tf_op | source)
XLA Modules:
  0.0 609.9 jit_solution(8935028124554305752)
XLA Ops:
  7.2 0.7 all-gather.5.cloned.1.call-update
  8.0 0.7 all-gather.3.cloned.1.call-update
  8.7 0.8 copy.33
  9.7 1.2 reduce-window.6
  11.4 0.7 multiply_add_fusion.1
  12.1 1.2 fusion.50
  13.4 3.9 convolution_convert_fusion.3
  17.3 8.2 %broadcast_in_dim.42 = bf16[32,4,24,2048]{3,2,1,0:T(8,128)(2,1)} broadcast(bf16[32,24,2048]{2,1,0:T(8,128)(2,1)} %bitcast.95), dimensions={0,2,3} | broadcast | bytes 15728640 | tf_op jit(solution)/shard_map/broadcast_in_dim | solution.py:179
  25.5 11.9 %all-to-all-start = ((bf16[128,24,2048]{2,1,0:T(8,128)(2,1)}), bf16[128,24,2048]{2,1,0:T(8,128)(2,1)}, u32[]{:S(2)}, u32[]{:S(2)}) async-start(bf16[128,24,2048]{2,1,0:T(8,128)(2,1)} %bitcast.91), calls=%async_computation.1 | async-start | bytes 25165824 | tf_op jit(solution)/shard_map/all_to_all | solution.py:183
  37.4 156.9 %all_gather.10 = bf16[512,512]{1,0:T(8,128)(2,1)S(1)} all-gather(bf16[128,512]{1,0:T(8,128)(2,1)S(1)} %copy-done.6), channel_id=1, replica_groups=mesh['ep'=32,'tp'=4] {'tp'}, dimensions={0}, use_global_device_ids=true | all-gather | bytes 655360 | tf_op jit(solution)/shard_map/all_gather | solution.py:68
  195.7 1.2 all-to-all-done
  196.9 9.7 %fusion.56 = f32[3072,256]{1,0:T(8,128)} fusion(bf16[3072,2048]{1,0:T(8,128)(2,1)} %bitcast.17, bf16[1,2048,256]{2,1,0:T(8,128)(2,1)S(1)} %copy-done.9), kind=kOutput, calls=%fused_computation.90 | convolution fusion | flops 3221225472 | bytes 16777216 | tf_op jit(solution)/shard_map/dot_general | solution.py:186
  206.5 19.1 %convolution_convert_fusion.2 = bf16[3072,2048]{1,0:T(8,128)(2,1)} fusion(bf16[3072,2048]{1,0:T(8,128)(2,1)} %bitcast.17, f32[3072,256]{1,0:T(8,128)} %fusion.56, bf16[1,256,2048]{2,1,0:T(8,128)(2,1)S(1)} %copy-done, bf16[1,2048,256]{2,1,0:T(8,128)(2,1)} %param.36), kind=kOutput, calls=%fused_computation.63 | convolution fusion | flops 6453460992 | bytes 30408704 | tf_op jit(solution)/shard_map/dot_general | solution.py:189
  225.6 15.1 %all-to-all-start.1 = ((bf16[128,24,2048]{2,1,0:T(8,128)(2,1)}), bf16[128,24,2048]{2,1,0:T(8,128)(2,1)}, u32[]{:S(2)}, u32[]{:S(2)}) async-start(bf16[128,24,2048]{2,1,0:T(8,128)(2,1)} %bitcast.94), calls=%async_computation.2 | async-start | bytes 25165824 | tf_op jit(solution)/shard_map/all_to_all | solution.py:192
  241.1 17.0 %all-gather.3.cloned.1.call-done = bf16[16384,256]{1,0:T(8,128)(2,1)} async-done(((bf16[128,256]{1,0:T(8,128)(2,1)}), bf16[16384,256]{1,0:T(8,128)(2,1)}) %all-gather.3.cloned.1.call-update) | async-done | bytes 8388624 | tf_op jit(solution)/shard_map/all_gather | solution.py:89
  258.2 57.2 %while.17 = (s32[]{:T(128)}, f32[4,512]{1,0:T(4,128)S(1)}, f32[4,512]{1,0:T(4,128)S(1)}, f32[4,512,64]{1,2,0:T(8,128)S(1)}, s32[32]{0:T(128)S(1)}, /*index=5*/s3...) while((s32[]{:T(128)}, f32[4,512]{1,0:T(4,128)S(1)}, ...), condition=%wide.region_7.8_spmd.clone, body=%wide.region_1.7_spmd.clone.sunk | while | flops 482656832 | bytes 25966364 | solution.py:136
  259.4 9.0 %conditional.3 = ((f32[4,512]{1,0:T(4,128)S(1)}, f32[4,512]{1,0:T(4,128)S(1)}, f32[4,512,64]{1,2,0:T(8,128)S(1)})) conditional(s32[]{:T(128)} %convert_element_type.193, (f32[4,512]{1,0:T(4,128)S(1)}, f32[4,512]{1,0:T(4,128)S(1)}, f32[4,512,64]{1,2,0:T(8,128)S(1)}) %tuple.59, (s32[]{:T(128)}, s32[512]{0:T(512)S(1)}, bf16[16384,256]{1,0:T(8,128)(2,1)}, ...), branch_computations={%region_2.2_spmd, %region_3.6_spmd} | conditional | flops 482649632 | bytes 25957090 | solution.py:131
  259.4 1.1 fusion.14
  260.6 1.3 convolution_convert_fusion.1
  261.9 0.8 fusion.88
  262.6 0.9 dynamic-slice_convert_fusion
  264.0 1.2 fusion.87
  265.2 0.8 fusion.5
  266.0 1.3 convolution_convert_fusion
  267.3 1.0 fusion.11
  269.6 9.0 %conditional.3 = ((f32[4,512]{1,0:T(4,128)S(1)}, f32[4,512]{1,0:T(4,128)S(1)}, f32[4,512,64]{1,2,0:T(8,128)S(1)})) conditional(s32[]{:T(128)} %convert_element_type.193, (f32[4,512]{1,0:T(4,128)S(1)}, f32[4,512]{1,0:T(4,128)S(1)}, f32[4,512,64]{1,2,0:T(8,128)S(1)}) %tuple.59, (s32[]{:T(128)}, s32[512]{0:T(512)S(1)}, bf16[16384,256]{1,0:T(8,128)(2,1)}, ...), branch_computations={%region_2.2_spmd, %region_3.6_spmd} | conditional | flops 482649632 | bytes 25957090 | solution.py:131
  269.6 1.1 fusion.14
  270.7 1.3 convolution_convert_fusion.1
  272.1 0.8 fusion.88
  272.8 0.9 dynamic-slice_convert_fusion
  274.2 1.2 fusion.87
  275.4 0.8 fusion.5
  276.2 1.3 convolution_convert_fusion
  277.5 1.0 fusion.11
  279.8 0.6 dynamic_slice.20
  283.5 0.6 dynamic_slice.20
  287.2 0.6 dynamic_slice.20
  290.9 0.6 dynamic_slice.20
  292.1 0.6 dynamic_slice.20
  295.8 0.6 dynamic_slice.20
  315.5 2.1 convolution_convert_fusion.4
  317.7 84.1 %all-to-all-done.1 = bf16[128,24,2048]{2,1,0:T(8,128)(2,1)} async-done(((bf16[128,24,2048]{2,1,0:T(8,128)(2,1)}), bf16[128,24,2048]{2,1,0:T(8,128)(2,1)}, u32[]{:S(2)}, u32[]{:S(2)}) %all-to-all-start.1) | async-done | bytes 12582944 | tf_op jit(solution)/shard_map/all_to_all | solution.py:192
  401.8 10.4 %bitcast_reduce_fusion = bf16[32,24,2048]{2,1,0:T(8,128)(2,1)} fusion(bf16[128,24,2048]{2,1,0:T(8,128)(2,1)} %all-to-all-done.1), kind=kLoop, calls=%fused_computation.62 | loop fusion | flops 4718592 | bytes 15728640 | tf_op jit(solution)/shard_map/reduce_sum | solution.py:201
  412.1 2.7 convolution_multiply_fusion.2
  415.0 0.6 convolution_multiply_fusion.3
  415.6 0.7 convolution_multiply_fusion.1
  416.3 1.6 fusion.45
  417.9 185.5 %reduce-scatter.2.cloned.1.call-done = bf16[128,2048]{1,0:T(8,128)(2,1)} async-done(((bf16[512,2048]{1,0:T(8,128)(2,1)}), bf16[128,2048]{1,0:T(8,128)(2,1)}) %reduce-scatter.2.cloned.1.call-update) | async-done | bytes 524304 | tf_op jit(solution)/shard_map/reduce_scatter | solution.py:150
  (259 shorter events, 19.6 us)
Async XLA Ops:
  7.2 199.4 %copy-start = (bf16[1,256,2048]{2,1,0:T(8,128)(2,1)S(1)}, bf16[1,256,2048]{2,1,0:T(8,128)(2,1)}, u32[]{:S(2)}) copy-start(bf16[1,256,2048]{2,1,0:T(8,128)(2,1)} %param.37) | copy-start | bytes 3145732
  7.2 233.9 %all-gather.5.cloned.1.call-start = ((), (), s32[]{:S(2)}) async-start(), calls=%async_computation.4 | async-start | bytes 1056768 | tf_op jit(solution)/shard_map/all_gather | solution.py:90
  7.9 250.1 %all-gather.3.cloned.1.call-start = ((), (), s32[]{:S(2)}) async-start(), calls=%async_computation.3 | async-start | bytes 8454144 | tf_op jit(solution)/shard_map/all_gather | solution.py:89
  25.5 12.0 %copy-start.6 = (bf16[128,512]{1,0:T(8,128)(2,1)S(1)}, bf16[128,512]{1,0:T(8,128)(2,1)}, u32[]{:S(2)}) copy-start(bf16[128,512]{1,0:T(8,128)(2,1)} %param.21) | copy-start | bytes 393220
  25.5 169.2 %copy-start.11 = (bf16[512,128]{1,0:T(8,128)(2,1)S(1)}, bf16[512,128]{1,0:T(8,128)(2,1)}, u32[]{:S(2)}) copy-start(bf16[512,128]{1,0:T(8,128)(2,1)} %param.27) | copy-start | bytes 393220
  25.5 169.2 %copy-start.12 = (f32[512]{0:T(512)S(1)}, f32[512]{0:T(512)}, u32[]{:S(2)}) copy-start(f32[512]{0:T(512)} %param.24) | copy-start | bytes 6148
  25.5 169.7 %copy-start.10 = (bf16[512,256]{1,0:T(8,128)(2,1)S(1)}, bf16[512,256]{1,0:T(8,128)(2,1)}, u32[]{:S(2)}) copy-start(bf16[512,256]{1,0:T(8,128)(2,1)} %param.26) | copy-start | bytes 786436
  25.5 171.4 %all-to-all-start = ((bf16[128,24,2048]{2,1,0:T(8,128)(2,1)}), bf16[128,24,2048]{2,1,0:T(8,128)(2,1)}, u32[]{:S(2)}, u32[]{:S(2)}) async-start(bf16[128,24,2048]{2,1,0:T(8,128)(2,1)} %bitcast.91), calls=%async_computation.1 | async-start | bytes 25165824 | tf_op jit(solution)/shard_map/all_to_all | solution.py:183
  37.4 159.5 %copy-start.9 = (bf16[1,2048,256]{2,1,0:T(8,128)(2,1)S(1)}, bf16[1,2048,256]{2,1,0:T(8,128)(2,1)}, u32[]{:S(2)}) copy-start(bf16[1,2048,256]{2,1,0:T(8,128)(2,1)} %param.35) | copy-start | bytes 3145732
  225.6 32.5 %copy-start.3 = (bf16[256,256]{1,0:T(8,128)(2,1)S(1)}, bf16[256,256]{1,0:T(8,128)(2,1)}, u32[]{:S(2)}) copy-start(bf16[256,256]{1,0:T(8,128)(2,1)} %param.28) | copy-start | bytes 393220
  225.6 32.5 %copy-start.4 = (bf16[256,256]{1,0:T(8,128)(2,1)S(1)}, bf16[256,256]{1,0:T(8,128)(2,1)}, u32[]{:S(2)}) copy-start(bf16[256,256]{1,0:T(8,128)(2,1)} %param.29) | copy-start | bytes 393220
  225.6 32.5 %copy-start.7 = (f32[256]{0:T(256)S(1)}, f32[256]{0:T(256)}, u32[]{:S(2)}) copy-start(f32[256]{0:T(256)} %param.25) | copy-start | bytes 3076
  225.6 176.1 %all-to-all-start.1 = ((bf16[128,24,2048]{2,1,0:T(8,128)(2,1)}), bf16[128,24,2048]{2,1,0:T(8,128)(2,1)}, u32[]{:S(2)}, u32[]{:S(2)}) async-start(bf16[128,24,2048]{2,1,0:T(8,128)(2,1)} %bitcast.94), calls=%async_computation.2 | async-start | bytes 25165824 | tf_op jit(solution)/shard_map/all_to_all | solution.py:192
  240.8 362.6 %reduce-scatter.2.cloned.1.call-start = ((), (), s32[]{:S(2)}) async-start(), calls=%async_computation.5 | async-start | bytes 2621440 | tf_op jit(solution)/shard_map/reduce_scatter | solution.py:150
  258.2 57.3 %copy-start.5 = (bf16[256,2048]{1,0:T(8,128)(2,1)S(1)}, bf16[256,2048]{1,0:T(8,128)(2,1)}, u32[]{:S(2)}) copy-start(bf16[256,2048]{1,0:T(8,128)(2,1)} %param.30) | copy-start | bytes 3145732
  315.4 2.2 copy-start.8
  412.1 2.8 copy-start.2
  415.6 187.8 %copy-start.1 = (bf16[1,256,2048]{2,1,0:T(8,128)(2,1)S(1)}, bf16[1,256,2048]{2,1,0:T(8,128)(2,1)}, u32[]{:S(2)}) copy-start(bf16[1,256,2048]{2,1,0:T(8,128)(2,1)} %param.37) | copy-start | bytes 3145732
Sparse Core Ops, SparseCore 0:
  10.8 144.9 all-gather.4
  159.0 99.0 all-gather.2
  317.8 285.5 reduce-scatter.1
where the time goes:
time: 616 us; the launch traced here: 610 us
  waiting for transfers between devices  289 us (47%)
  blocking collectives  157 us (25%)
  matrix products  52.5 us (9%)
  local copies, waits for them, and re-layouts  27.9 us (5%)
  starting transfers between devices  27.4 us (4%)
  other arithmetic  21.3 us (3%)
  loops' own time  20.8 us (3%)
  between operations  14 us (2%)
    reduce_scatter x1, waiting for transfers between devices, on_device(): lax.psum_scatter(lax.optimization_barrier(partial_out).astype(jnp.float32...  185 us
    all_gather x1, blocking collectives, on_device(): shard_rows = lax.all_gather(q_latent, 'tp', axis=0, tiled=True)  157 us
    all_to_all x1, waiting for transfers between devices, on_device(): lax.all_to_all(partial_out.reshape(sources, item_count, feature_width), (...  84.1 us
    another operation x1, loops' own time, on_device(): lax.scan(key_step, start_state, jnp.arange(shard_count // grouping, dtype...  20.2 us
    dot_general x1, matrix products, on_device(): jnp.dot(hidden, down_weight, preferred_element_type=jnp.float32)  19.1 us
    dynamic_slice x32, local copies, waits for them, and re-layouts, on_device(): lax.scan(key_step, start_state, jnp.arange(shard_count // grouping, dtype...  17.9 us
    all_gather x1, waiting for transfers between devices, on_device(): latents = lax.all_gather(kv_latent, ('ep', 'tp'), axis=0, tiled=True)  17 us
    all_to_all x1, starting transfers between devices, on_device(): lax.all_to_all(partial_out.reshape(sources, item_count, feature_width), (...  15.1 us
  transfers between devices with their start and end apart: 5, of which 4 were waited for; matrix products, arithmetic and copies ran while one was open for 17% of the time, Pallas kernels for 0%

commit v1 on v0

v1 whole, which is shorter than its diff:
```python
import math

import jax
import jax.numpy as jnp
from jax import lax
from jax.experimental import pallas as pl
from jax.experimental.pallas import tpu as pltpu
from jax.sharding import PartitionSpec as P


D = 2048
NOPE = 64
ROPE = 32
TOPK = 4

norm_epsilon = 1e-06
rope_base = 10000.0
masked_score = -1e30


KEYS = 512
QUERIES = 256
HEADS_HERE = 4
STEPS_A_CHUNK = 4
PIECE = 256
excess_limit = 60.0
exponent_scale = (NOPE + ROPE) ** (-0.5) * math.log2(math.e)

BY_LAST = (((1,), (1,)), ((), ()))
BY_FIRST = (((0,), (0,)), ((), ()))


def rms_scale(values_in, gain_vec):
    floats = values_in.astype(jnp.float32)
    return (
        floats
        * lax.rsqrt(jnp.mean(floats * floats, axis=-1, keepdims=True) + norm_epsilon)
        * gain_vec
    )


def tables(positions):
    half_width = ROPE // 2
    frequency = rope_base ** (-jnp.arange(half_width, dtype=jnp.float32) / half_width)
    angles = positions.astype(jnp.float32)[:, None] * frequency[None, :]
    return (jnp.cos(angles), jnp.sin(angles))


def rotate_pairs(values_in, cosine, sine_table):
    half_width = values_in.shape[-1] // 2
    first, second = (values_in[..., :half_width], values_in[..., half_width:])
    return jnp.concatenate(
        [first * cosine - second * sine_table, first * sine_table + second * cosine], axis=-1
    )


def attention_kernel(
    place_ref,
    kv_ref,
    q_ref,
    wq_ref,
    wr_ref,
    cos_ref,
    sin_ref,
    wk_ref,
    wv_ref,
    wo_ref,
    after_ref,
    out_ref,
    held_ref,
    query_ref,
    pair_ref,
    vt_ref,
    max_ref,
    sum_ref,
    excess_ref,
    sem,
):
    group = place_ref[0]
    last = place_ref[1]
    low = 31 - last
    chunk = 4 * STEPS_A_CHUNK
    chunks = 32 // STEPS_A_CHUNK
    copies = [
        pltpu.make_async_copy(
            kv_ref.at[pl.ds(n * chunk, chunk)], held_ref.at[pl.ds(n * chunk, chunk)], sem.at[n]
        )
        for n in range(chunks)
    ]
    for copy in copies:
        copy.start()

    for half in range(2):
        rows = jnp.concatenate(
            [
                jnp.concatenate(
                    [
                        q_ref[half, place_ref[2 + t], n * 64 : n * 64 + 64]
                        for n in range(4)
                    ],
                    axis=1,
                )
                for t in range(4)
            ],
            axis=0,
        )
        plain = lax.dot_general(
            wq_ref[...], rows, BY_LAST, preferred_element_type=jnp.float32
        ).astype(jnp.bfloat16)
        turned = lax.dot_general(wr_ref[...], rows, BY_LAST, preferred_element_type=jnp.float32)
        cosine, sine = cos_ref[half], sin_ref[half]
        for h in range(HEADS_HERE):
            first = turned[h * 32 : h * 32 + 16]
            second = turned[h * 32 + 16 : h * 32 + 32]
            at = (h % 2) * 64
            query_ref[half, h, at : at + 64] = plain[h * 64 : h * 64 + 64]
            query_ref[half, h, 64 - at : 128 - at] = jnp.zeros((64, QUERIES), jnp.bfloat16)
            query_ref[half, h, 128:144] = (first * cosine - second * sine).astype(jnp.bfloat16)
            query_ref[half, h, 144:160] = (first * sine + second * cosine).astype(jnp.bfloat16)
            query_ref[half, h, 160:256] = jnp.zeros((96, QUERIES), jnp.bfloat16)
    for h in range(HEADS_HERE):
        vt_ref[h, 64:80] = jnp.ones((16, KEYS), jnp.bfloat16)

    def clear():
        max_ref[...] = jnp.full_like(max_ref, masked_score)
        sum_ref[...] = jnp.zeros_like(sum_ref)

    def project(j):
        base = j * 4
        normed_rows, rope_rows = [], []
        for t in range(4):
            at = base + place_ref[2 + t]
            normed_rows.append(
                jnp.concatenate([held_ref[at, 0:128], held_ref[at, 128:256]], axis=1)
            )
            packed = held_ref[at, 256:288].astype(jnp.float32)
            for k in range(4):
                rope_rows.append(
                    (packed if k == 0 else pltpu.roll(packed, 128 - 32 * k, 1)).astype(jnp.bfloat16)
                )
        normed = jnp.concatenate(normed_rows, axis=0)
        rope = jnp.concatenate(rope_rows, axis=0)
        keys = jnp.dot(normed, wk_ref[...], preferred_element_type=jnp.float32).astype(jnp.bfloat16)
        vals = lax.dot_general(
            wv_ref[...], normed, BY_LAST, preferred_element_type=jnp.float32
        ).astype(jnp.bfloat16)
        for p in range(2):
            pair_ref[p, :, 0:128] = keys[:, p * 128 : p * 128 + 128]
            pair_ref[p, :, 128:256] = rope
        for h in range(HEADS_HERE):
            vt_ref[h, 0:64] = vals[h * 64 : h * 64 + 64]

    def hidden_keys(j, half):
        edge = jnp.where(half == 0, group, 31 - group)
        key_segment = lax.broadcasted_iota(jnp.int32, (KEYS, QUERIES), 0) // 64 + 8 * j
        query_segment = (
            2 * (lax.broadcasted_iota(jnp.int32, (KEYS, QUERIES), 1) // 64) + half + 8 * edge
        )
        return key_segment > query_segment

    def safe_tile(j, half):
        hidden = hidden_keys(j, half)
        for h in range(HEADS_HERE):
            scores = jnp.dot(
                pair_ref[h // 2], query_ref[half, h], preferred_element_type=jnp.float32
            )
            scores = jnp.where(hidden, masked_score, scores)
            old = max_ref[half, h, 0:1]
            new = jnp.maximum(old, jnp.max(scores, axis=0, keepdims=True))
            factor = jnp.exp2((old - new) * exponent_scale)
            weights = jnp.exp2((scores - new) * exponent_scale).astype(jnp.bfloat16)
            part = jnp.dot(vt_ref[h], weights, preferred_element_type=jnp.float32)
            sum_ref[half, h] = sum_ref[half, h] * factor + part
            max_ref[half, h, 0:1] = new

    def tiles(j, halves, masked):
        units = [(half, h) for half in halves for h in range(HEADS_HERE)]
        hidden = hidden_keys(j, halves[0]) if masked else None
        count = len(units)
        base = [max_ref[half, h, 0:1] for half, h in units]
        peak, weights = [None] * count, [None] * count

        def weigh(u):
            half, h = units[u]
            tops, pieces = [], []
            for p in range(0, KEYS, PIECE):
                scores = jnp.dot(
                    pair_ref[h // 2, p : p + PIECE],
                    query_ref[half, h],
                    preferred_element_type=jnp.float32,
                )
                if masked:
                    scores = jnp.where(hidden[p : p + PIECE], masked_score, scores)
                tops.append(jnp.max(scores, axis=0, keepdims=True))
                pieces.append(
                    jnp.exp2((scores - base[u]) * exponent_scale).astype(jnp.bfloat16)
                )
            top = tops[0]
            for other in tops[1:]:
                top = jnp.maximum(top, other)
            peak[u] = top
            weights[u] = jnp.concatenate(pieces, axis=0)

        def gather(u):
            half, h = units[u]
            part = jnp.dot(vt_ref[h], weights[u], preferred_element_type=jnp.float32)
            new = jnp.maximum(base[u], peak[u])
            factor = jnp.exp2((base[u] - new) * exponent_scale)
            sum_ref[half, h] = (sum_ref[half, h] + part) * factor
            max_ref[half, h, 0:1] = new

        for u in range(count + 1):
            if u < count:
                weigh(u)
            if u:
                gather(u - 1)
        most = peak[0] - base[0]
        for u in range(1, count):
            most = jnp.maximum(most, peak[u] - base[u])
        excess_ref[0:1] = jnp.maximum(excess_ref[0:1], most)

    def safe_step(j):
        project(j)
        for half in range(2):
            edge = group if half == 0 else 31 - group

            @pl.when(j <= edge)
            def _():
                safe_tile(j, half)

    def one_half(j):
        for half in range(2):
            edge = group if half == 0 else 31 - group

            @pl.when(jnp.logical_and(j >= low, j < edge))
            def _():
                tiles(j, (half,), False)

            @pl.when(j == edge)
            def _():
                tiles(j, (half,), True)

    clear()
    excess_ref[...] = jnp.zeros_like(excess_ref)
    copies[0].wait()
    lax.fori_loop(0, 1, lambda j, c: (safe_step(j), c)[1], 0)

    def step(j, carried):
        for n in range(1, chunks):

            @pl.when(j == n * STEPS_A_CHUNK)
            def _():
                copies[n].wait()

        project(j)

        @pl.when(j < low)
        def _():
            tiles(j, (0, 1), False)

        @pl.when(j >= low)
        def _():
            one_half(j)

        return carried

    lax.fori_loop(1, last + 1, step, 0)
    for n in range(1, chunks):

        @pl.when(last < n * STEPS_A_CHUNK)
        def _():
            copies[n].wait()

    worst = jnp.max(excess_ref[0:1]) * exponent_scale

    @pl.when(jnp.logical_not(worst < excess_limit))
    def _():
        clear()
        lax.fori_loop(0, last + 1, lambda j, c: (safe_step(j), c)[1], 0)

    for half in range(2):
        heads = [
            (sum_ref[half, h, 0:64] / sum_ref[half, h, 64:65]).astype(jnp.bfloat16)
            for h in range(HEADS_HERE)
        ]
        attended = jnp.concatenate(heads, axis=0)
        part = lax.dot_general(
            attended, wo_ref[...], BY_FIRST, preferred_element_type=jnp.float32
        ).astype(jnp.bfloat16)
        out_ref[:, half] = part.reshape(4, 64, D)


def attention(place, kv, q, wq_t, wr_t, cosine, sine, wk, wv_t, wo, after):
    return pl.pallas_call(
        attention_kernel,
        in_specs=[
            pl.BlockSpec(memory_space=pltpu.SMEM),
            pl.BlockSpec(memory_space=pl.ANY),
        ]
        + [pl.BlockSpec(memory_space=pltpu.VMEM)] * 8
        + [pl.BlockSpec(memory_space=pl.ANY)],
        out_specs=pl.BlockSpec(memory_space=pltpu.VMEM),
        scratch_shapes=[
            pltpu.VMEM((128, 288, 128), jnp.bfloat16),
            pltpu.VMEM((2, HEADS_HERE, 256, QUERIES), jnp.bfloat16),
            pltpu.VMEM((2, KEYS, 256), jnp.bfloat16),
            pltpu.VMEM((HEADS_HERE, 80, KEYS), jnp.bfloat16),
            pltpu.VMEM((2, HEADS_HERE, 8, QUERIES), jnp.float32),
            pltpu.VMEM((2, HEADS_HERE, 80, QUERIES), jnp.float32),
            pltpu.VMEM((8, QUERIES), jnp.float32),
            pltpu.SemaphoreType.DMA((32 // STEPS_A_CHUNK,)),
        ],
        out_shape=jax.ShapeDtypeStruct((4, 2, 64, D), jnp.bfloat16),
        cost_estimate=pl.CostEstimate(
            flops=30_000_000_000, bytes_accessed=16_000_000, transcendentals=17_000_000
        ),
        name="attention",
    )(place, kv, q, wq_t, wr_t, cosine, sine, wk, wv_t, wo, after)


ROWS = 256
COLUMNS = 512


def experts_kernel(pieces, carried, x_ref, *refs):
    total_pieces = sum(sum(block) for block in pieces)
    parts = refs[:total_pieces]
    refs = refs[total_pieces + 1 :]
    before_ref = None
    if carried:
        before_ref, refs = refs[0], refs[1:]
    out_ref = refs[0]
    held = refs[1 : 1 + 3 * len(pieces)]
    sem = refs[1 + 3 * len(pieces)]
    copies, n = [], 0
    for b, block in enumerate(pieces):
        for role, number in enumerate(block):
            target, own = held[3 * b + role], []
            for piece in range(number):
                rows = target.shape[0] // number
                own.append(
                    pltpu.make_async_copy(
                        parts[n], target.at[pl.ds(piece * rows, rows)], sem.at[n]
                    )
                )
                n += 1
            copies.append(own)
    first_step = pl.program_id(0) == 0

    @pl.when(first_step)
    def _():
        for own in copies:
            for copy in own:
                copy.start()

    def ready(n):
        @pl.when(first_step)
        def _():
            for copy in copies[n]:
                copy.wait()

    rows = x_ref[...]
    hidden = []
    for b in range(len(pieces)):
        ready(3 * b)
        gate_part = jnp.dot(rows, held[3 * b][...], preferred_element_type=jnp.float32)
        ready(3 * b + 1)
        up_part = jnp.dot(rows, held[3 * b + 1][...], preferred_element_type=jnp.float32)
        hidden.append((jax.nn.silu(gate_part) * up_part).astype(jnp.bfloat16))
    for b in range(len(pieces)):
        ready(3 * b + 2)
    for n in range(0, D, COLUMNS):
        total = before_ref[:, n : n + COLUMNS] if carried else None
        for b in range(len(pieces)):
            part = jnp.dot(
                hidden[b], held[3 * b + 2][:, n : n + COLUMNS], preferred_element_type=jnp.float32
            )
            part = part.astype(jnp.bfloat16).astype(jnp.float32)
            total = part if total is None else total + part
        out_ref[:, n : n + COLUMNS] = total.astype(out_ref.dtype)


def experts(rows, blocks, before, after, out_type):
    pieces = [[len(role) for role in block] for block in blocks]
    flat = [piece for block in blocks for role in block for piece in role]
    whole = [
        pltpu.VMEM((len(role) * role[0].shape[0], role[0].shape[1]), jnp.bfloat16)
        for block in blocks
        for role in block
    ]
    count = len(blocks)
    apart = pl.BlockSpec(memory_space=pl.ANY)
    by_rows = pl.BlockSpec((ROWS, D), lambda r: (r, 0))
    operands = [rows, *flat, after]
    in_specs = [by_rows] + [apart] * (len(flat) + 1)
    if before is not None:
        operands.append(before)
        in_specs.append(by_rows)

    def body(*refs):
        experts_kernel(pieces, before is not None, *refs)

    return pl.pallas_call(
        body,
        grid=(rows.shape[0] // ROWS,),
        in_specs=in_specs,
        out_specs=by_rows,
        out_shape=jax.ShapeDtypeStruct(rows.shape, out_type),
        scratch_shapes=whole + [pltpu.SemaphoreType.DMA((len(flat),))],
        compiler_params=pltpu.CompilerParams(dimension_semantics=("arbitrary",)),
        cost_estimate=pl.CostEstimate(
            flops=2 * rows.shape[0] * D * 768 * count,
            bytes_accessed=3_000_000 * count + 12_000_000,
            transcendentals=rows.shape[0] * 256 * count,
        ),
    )(*operands)


def layer(
    q_latent,
    kv_latent,
    rope_key,
    q_gain,
    kv_gain,
    w_query,
    w_query_rot,
    w_key,
    w_value,
    w_mix_out,
    expert_input,
    ffn_gain,
    expert_ids,
    route_weights,
    w_gate_exp,
    w_up_exp,
    w_down_exp,
):
    both = ("ep", "tp")
    tok_rows = q_latent.shape[0]
    ep_count = lax.axis_size("ep")
    tp_count = lax.axis_size("tp")
    group_rows = tp_count * tok_rows
    ep = lax.axis_index("ep")
    tp = lax.axis_index("tp")
    own_start = ep * group_rows + tp * tok_rows

    def shift(by):
        return [
            (e * tp_count + t, e * tp_count + (t + by) % tp_count)
            for e in range(ep_count)
            for t in range(tp_count)
        ]

    mirror = [
        (e * tp_count + t, (ep_count - 1 - e) * tp_count + t)
        for e in range(ep_count)
        for t in range(tp_count)
    ]

    half_rows = tok_rows // 2
    kv_normed = rms_scale(kv_latent, kv_gain).astype(jnp.bfloat16)
    cosine, sine = tables(own_start + jnp.arange(tok_rows, dtype=jnp.int32))
    k_turned = rotate_pairs(rope_key.astype(jnp.float32), cosine, sine).astype(jnp.bfloat16)
    k_packed = jnp.concatenate([k_turned[k * 32 : k * 32 + 32] for k in range(4)], axis=1)
    q_normed = rms_scale(q_latent, q_gain).astype(jnp.bfloat16)
    q_packed = [
        q_normed[half * half_rows : half * half_rows + half_rows, n * 128 : n * 128 + 128]
        for half in range(2)
        for n in range(4)
    ]
    own = jnp.concatenate([kv_normed[:, :128], kv_normed[:, 128:], k_packed, *q_packed], axis=0)
    group = jnp.stack(
        [
            own,
            lax.ppermute(own, both, shift(1)),
            lax.ppermute(own, both, shift(-1)),
            lax.ppermute(own, both, shift(2)),
        ]
    )
    kv_rows = 2 * tok_rows + 32
    kv_all = lax.all_gather(group[:, :kv_rows], "ep", axis=0, tiled=True)
    behind = (jnp.arange(tp_count, dtype=jnp.int32) - tp) % tp_count
    order = jnp.where(behind == 0, 0, jnp.where(behind == 3, 1, jnp.where(behind == 1, 2, 3)))
    place = jnp.concatenate(
        [jnp.stack([ep, jnp.maximum(ep, ep_count - 1 - ep)]), order]
    ).astype(jnp.int32)

    q_mirrored = lax.ppermute(group[:, kv_rows + tok_rows * 2 :], both, mirror)
    q_both = jnp.stack([group[:, kv_rows : kv_rows + tok_rows * 2], q_mirrored])
    spread = (
        jnp.arange(tp_count, dtype=jnp.int32)[:, None] * tok_rows
        + jnp.arange(half_rows, dtype=jnp.int32)[None, :]
    ).reshape(-1)
    q_positions = jnp.concatenate(
        [ep * group_rows + spread, (ep_count - 1 - ep) * group_rows + half_rows + spread]
    )
    q_cosine, q_sine = tables(q_positions)
    q_cosine = q_cosine.reshape(2, QUERIES, ROPE // 2).transpose(0, 2, 1)
    q_sine = q_sine.reshape(2, QUERIES, ROPE // 2).transpose(0, 2, 1)

    gate, up, down = w_gate_exp[0], w_up_exp[0], w_down_exp[0]
    half_units = down.shape[0] // 2
    gate_left = lax.ppermute(gate, both, shift(1))
    gate_right = lax.ppermute(gate, both, shift(-1))
    up_left = lax.ppermute(up, both, shift(1))
    up_right = lax.ppermute(up, both, shift(-1))
    down_left = lax.ppermute(down, both, shift(1))
    down_right = lax.ppermute(down, both, shift(-1))
    gate_across = lax.ppermute(gate_left, both, shift(1))
    up_across = lax.ppermute(up_right, both, shift(-1))
    down_across = [
        lax.ppermute(down_left[:half_units], both, shift(1)),
        lax.ppermute(down_right[half_units:], both, shift(-1)),
    ]

    expert_count = ep_count
    slot_count = 3 * tok_rows * TOPK // (2 * expert_count)
    normed = rms_scale(expert_input, ffn_gain).astype(jnp.bfloat16)
    routed = expert_ids.reshape(-1)
    onehot = (routed[:, None] == jnp.arange(expert_count, dtype=jnp.int32)[None, :]).astype(
        jnp.int32
    )
    slot_number = jnp.sum((jnp.cumsum(onehot, axis=0) - 1) * onehot, axis=-1)
    slot_place = (routed * slot_count + slot_number).reshape(tok_rows, TOPK)
    slot_line = jnp.arange(expert_count * slot_count, dtype=jnp.int32)
    picks = [
        (slot_place[:, route_rank][:, None] == slot_line[None, :]).astype(jnp.bfloat16)
        for route_rank in range(TOPK)
    ]
    dispatch = picks[0]
    for route_rank in range(1, TOPK):
        dispatch = dispatch + picks[route_rank]
    outgoing = lax.dot_general(
        dispatch, normed, BY_FIRST, preferred_element_type=jnp.float32
    ).astype(jnp.bfloat16)
    slot_weights = sum(
        jnp.where(
            slot_place[:, route_rank][:, None] == slot_line[None, :],
            route_weights[:, route_rank : route_rank + 1],
            0.0,
        )
        for route_rank in range(TOPK)
    )
    coarse = slot_weights.astype(jnp.bfloat16)
    fine = (slot_weights - coarse.astype(jnp.float32)).astype(jnp.bfloat16)
    split_weights = jnp.concatenate([coarse, fine], axis=0)
    arrived = lax.all_to_all(
        outgoing.reshape(expert_count, slot_count, D),
        "ep",
        split_axis=0,
        concat_axis=0,
        tiled=True,
    )
    chosen = arrived.reshape(expert_count * slot_count, D)

    near = experts(
        chosen,
        [
            ([gate], [up], [down]),
            ([gate_left], [up_left], [down_left]),
            ([gate_right], [up_right], [down_right]),
        ],
        None,
        place,
        jnp.float32,
    )

    partial_out = attention(
        place,
        kv_all,
        q_both,
        w_query.T,
        w_query_rot.T,
        q_cosine,
        q_sine,
        w_key,
        w_value.T,
        w_mix_out,
        near,
    ).reshape(group_rows, D)
    mixed = lax.psum_scatter(partial_out, "tp", scatter_dimension=0, tiled=True)
    mixer_out = jnp.concatenate(
        [mixed[:half_rows], lax.ppermute(mixed[half_rows:], both, mirror)], axis=0
    )

    results = experts(
        chosen, [([gate_across], [up_across], down_across)], near, partial_out, jnp.bfloat16
    )
    returned = lax.all_to_all(
        results.reshape(expert_count, slot_count, D),
        "ep",
        split_axis=0,
        concat_axis=0,
        tiled=True,
    )
    returned = returned.reshape(expert_count * slot_count, D)

    fetched = jnp.dot(split_weights, returned, preferred_element_type=jnp.float32)
    expert_out = (fetched[:tok_rows] + fetched[tok_rows:]).astype(jnp.bfloat16)
    return (mixer_out, expert_out)


def solution(mesh):
    return jax.shard_map(
        layer,
        mesh=mesh,
        in_specs=(
            P(("ep", "tp"), None),
            P(("ep", "tp"), None),
            P(("ep", "tp"), None),
            P(),
            P(),
            P(None, "tp"),
            P(None, "tp"),
            P(None, "tp"),
            P(None, "tp"),
            P("tp", None),
            P(("ep", "tp"), None),
            P(),
            P(("ep", "tp"), None),
            P(("ep", "tp"), None),
            P("ep", None, "tp"),
            P("ep", None, "tp"),
            P("ep", "tp", None),
        ),
        out_specs=(P(("ep", "tp"), None), P(("ep", "tp"), None)),
        check_vma=False,
    )
```

time: 616 us -> 362 us (0.59)
  waiting for transfers between devices: 289 us -> 125 us
  blocking collectives: 157 us -> 0 us
  Pallas kernels: 0 us -> 141 us
  matrix products: 52.5 us -> 5.23 us
  loops' own time: 20.8 us -> 0 us
  starting transfers between devices: 27.4 us -> 43.9 us
  local copies, waits for them, and re-layouts: 27.9 us -> 13.7 us
    reduce_scatter x1, waiting for transfers between devices: 185 us -> 0.01 us  [layer(): mixed = lax.psum_scatter(partial_out, 'tp', scatter_dimension=0, tiled=True)]
    all_gather x1 -> x0, blocking collectives: 157 us -> none  [on_device(): shard_rows = lax.all_gather(q_latent, 'tp', axis=0, tiled=True)]
    pallas_call x0 -> x3, Pallas kernels: none -> 141 us  [the longest x1 111 us: attention(): pl.pallas_call(attention_kernel, in_specs=[pl.BlockSpec(memory_space=pltp...]
    ppermute x0 -> x15, waiting for transfers between devices: none -> 85.4 us  [the longest x1 37.8 us: layer(): q_mirrored = lax.ppermute(group[:, kv_rows + tok_rows * 2:], both, mirror)]
    dot_general x20 -> x2, matrix products: 52.5 us -> 5.23 us  [the longest x1 2.91 us: layer(): lax.dot_general(dispatch, normed, BY_FIRST, preferred_element_type=jnp.fl...]
    all_to_all x2, waiting for transfers between devices: 85.3 us -> 39.6 us  [the longest x1 39.6 us: layer(): lax.all_to_all(results.reshape(expert_count, slot_count, D), 'ep', split_...]
    ppermute x0 -> x15, starting transfers between devices: none -> 25.4 us  [the longest x1 5.42 us: layer(): q_mirrored = lax.ppermute(group[:, kv_rows + tok_rows * 2:], both, mirror)]
    another operation x33 -> x0, loops' own time: 20.8 us -> none  [the longest x1 20.2 us: on_device(): lax.scan(key_step, start_state, jnp.arange(shard_count // grouping, dtype...]
  transfers between devices with their start and end apart: 5 -> 19, of which waited for: 4 -> 9; matrix products, arithmetic and copies ran while one was open for 17% -> 7% of each run, Pallas kernels for 0% -> 39%
where the time goes in v1:
time: 362 us; the launch traced here: 359 us
  Pallas kernels  141 us (39%)
  waiting for transfers between devices  125 us (35%)
  starting transfers between devices  43.9 us (12%)
  other arithmetic  16 us (4%)
  between operations  14.5 us (4%)
  local copies, waits for them, and re-layouts  13.7 us (4%)
  matrix products  5.23 us (1%)
    pallas_call x1, Pallas kernels, attention(): pl.pallas_call(attention_kernel, in_specs=[pl.BlockSpec(memory_space=pltp...  111 us
    all_to_all x1, waiting for transfers between devices, layer(): lax.all_to_all(results.reshape(expert_count, slot_count, D), 'ep', split_...  39.6 us
    ppermute x1, waiting for transfers between devices, layer(): q_mirrored = lax.ppermute(group[:, kv_rows + tok_rows * 2:], both, mirror)  37.8 us
    pallas_call x2, Pallas kernels, experts(): pl.pallas_call(body, grid=(rows.shape[0] // ROWS,), in_specs=in_specs, ou...  30 us
    ppermute x1, waiting for transfers between devices, layer(): lax.ppermute(down_left[:half_units], both, shift(1))  13.3 us
    ppermute x1, waiting for transfers between devices, layer(): up_left = lax.ppermute(up, both, shift(1))  10.2 us
    all_to_all x1, starting transfers between devices, layer(): lax.all_to_all(outgoing.reshape(expert_count, slot_count, D), 'ep', split...  9.76 us
    all_to_all x1, starting transfers between devices, layer(): lax.all_to_all(results.reshape(expert_count, slot_count, D), 'ep', split_...  8.64 us
  transfers between devices with their start and end apart: 19, of which 9 were waited for; matrix products, arithmetic and copies ran while one was open for 7% of the time, Pallas kernels for 39%

profile of v1, /device:TPU:1, one launch (start us, length us, event | category | flops | bytes accessed | tf_op | source)
XLA Modules:
  0.0 359.4 jit_solution(16804851479947837383)
XLA Ops:
  7.3 0.8 convert_element_type.73
  8.6 1.0 fusion.30
  9.6 0.9 fusion.32
  10.6 1.0 fusion.16
  11.6 1.0 fusion.18
  12.8 2.1 collective-permute-start
  14.9 1.3 collective-permute-start.1
  16.3 1.6 collective-permute-start.2
  17.9 2.7 collective-permute-done
  20.6 5.6 %collective-permute-done.2 = bf16[800,128]{1,0:T(8,128)(2,1)S(1)} collective-permute-done((bf16[800,128]{1,0:T(8,128)(2,1)S(1)}, bf16[800,128]{1,0:T(8,128)(2,1)S(1)}, u32[]{:S(2)}, u32[]{:S(2)}) %collective-permute-start.2) | collective-permute-done | bytes 204832 | tf_op jit(solution)/shard_map/ppermute | solution.py:477
  26.9 0.7 slice.162
  28.1 1.2 reduce-window.6
  30.0 2.9 convolution_convert_fusion
  33.0 9.8 %all-to-all-start = ((bf16[32,24,2048]{2,1,0:T(8,128)(2,1)}), bf16[32,24,2048]{2,1,0:T(8,128)(2,1)S(1)}, u32[]{:S(2)}, u32[]{:S(2)}) async-start(bf16[32,24,2048]{2,1,0:T(8,128)(2,1)} %bitcast.16), calls=%async_computation | async-start | bytes 6291456 | tf_op jit(solution)/shard_map/all_to_all | solution.py:547
  42.8 0.9 collective-permute-start.4
  43.7 1.1 maximum_bitcast_fusion
  44.8 5.4 %collective-permute-start.3 = (bf16[4,256,128]{2,1,0:T(8,128)(2,1)S(1)}, bf16[4,256,128]{2,1,0:T(8,128)(2,1)}, u32[]{:S(2)}, u32[]{:S(2)}) collective-permute-start(bf16[4,256,128]{2,1,0:T(8,128)(2,1)S(1)} %get-tuple-element.3), channel_id=1, source_target_pairs={{0,124},{1,125},{2,126},{3,127},{4,120},{5,121},{6,122},{7,123},{8... | collective-permute-start | bytes 786440 | tf_op jit(solution)/shard_map/ppermute | solution.py:488
  50.2 2.7 collective-permute-start.9
  53.5 37.8 %collective-permute-done.3 = bf16[4,256,128]{2,1,0:T(8,128)(2,1)} collective-permute-done((bf16[4,256,128]{2,1,0:T(8,128)(2,1)S(1)}, bf16[4,256,128]{2,1,0:T(8,128)(2,1)}, u32[]{:S(2)}, u32[]{:S(2)}) %collective-permute-start.3) | collective-permute-done | bytes 262176 | tf_op jit(solution)/shard_map/ppermute | solution.py:488
  92.0 2.0 collective-permute-start.7
  95.3 0.7 fusion.47
  96.1 1.8 copy.57
  97.9 0.8 copy.59
  98.6 1.7 copy.58
  100.9 1.5 multiply_sine_fusion
  102.4 1.8 pad_maximum_fusion.1.q_ref
  104.2 2.7 collective-permute-start.12
  106.9 10.2 %collective-permute-done.5.refs_5_ = bf16[2048,256]{1,0:T(8,128)(2,1)} collective-permute-done((bf16[2048,256]{1,0:T(8,128)(2,1)}, bf16[2048,256]{1,0:T(8,128)(2,1)}, u32[]{:S(2)}, u32[]{:S(2)}) %collective-permute-start.5) | collective-permute-done | bytes 1048608 | tf_op jit(solution)/shard_map/ppermute | solution.py:505
  117.1 3.5 collective-permute-done.7.refs_7_
  120.7 1.6 copy-done
  122.3 19.6 %shard_map.176.after_ref.refs_6_ = f32[768,2048]{1,0:T(8,128)} custom-call(bf16[768,2048]{1,0:T(8,128)(2,1)} %bitcast.53, bf16[2048,256]{1,0:T(8,128)(2,1)} %bitcast.71, bf16[2048,256]{1,0:T(8,128)(2,1)} %bitcast.74, bf16[256,2048]{1,0:T(8,128)(2,1)} %bitcast.77, bf16[2048,256]{1,0:T(8,128)(2,1)} %collective-permute-done.4.refs_4_, ...), custom_call_target="tpu_custom_call" | custom-call | flops 7247757312 | bytes 21000000 | tf_op jit(solution)/shard_map/pallas_call | solution.py:403
  141.9 111.0 %attention.1 = bf16[4,2,64,2048]{3,2,1,0:T(8,128)(2,1)} custom-call(s32[6]{0:T(128)} %pad_add_fusion.refs_10_.place_ref, bf16[128,288,128]{2,1,0:T(8,128)(2,1)} %all-gather.2.cloned.1.call-done.kv_ref, bf16[2,4,256,128]{3,2,1,0:T(8,128)(2,1)} %pad_maximum_fusion.1.q_ref, bf16[256,512]{1,0:T(8,128)(2,1)} %bitcast.66, bf16[128,512]{1,0:T(8,128)(2,1)} %bitcast.68, ...), custom_call_target="tpu_custom_call" | custom-call | flops 30000001024 | bytes 16000000 | tf_op jit(solution)/shard_map/attention/pallas_call | solution.py:294
  253.0 1.1 slice.166
  254.0 1.3 collective-permute-start.13
  255.3 1.1 slice.167
  256.4 2.2 collective-permute-start.14
  258.6 13.3 %collective-permute-done.13.refs_3_ = bf16[128,2048]{1,0:T(8,128)(2,1)S(1)} collective-permute-done((bf16[128,2048]{1,0:T(8,128)(2,1)S(1)}, bf16[128,2048]{1,0:T(8,128)(2,1)S(1)}, u32[]{:S(2)}, u32[]{:S(2)}) %collective-permute-start.13) | collective-permute-done | bytes 524320 | tf_op jit(solution)/shard_map/ppermute | solution.py:512
  271.9 6.1 %collective-permute-done.14.refs_4_ = bf16[128,2048]{1,0:T(8,128)(2,1)S(1)} collective-permute-done((bf16[128,2048]{1,0:T(8,128)(2,1)S(1)}, bf16[128,2048]{1,0:T(8,128)(2,1)S(1)}, u32[]{:S(2)}, u32[]{:S(2)}) %collective-permute-start.14) | collective-permute-done | bytes 524320 | tf_op jit(solution)/shard_map/ppermute | solution.py:513
  278.0 0.8 copy-done.7
  278.8 10.5 %shard_map.177 = bf16[768,2048]{1,0:T(8,128)(2,1)} custom-call(bf16[768,2048]{1,0:T(8,128)(2,1)} %bitcast.54, bf16[2048,256]{1,0:T(8,128)(2,1)} %collective-permute-done.11.refs_1_, bf16[2048,256]{1,0:T(8,128)(2,1)} %collective-permute-done.12.refs_2_, bf16[128,2048]{1,0:T(8,128)(2,1)} %copy-done.6, bf16[128,2048]{1,0:T(8,128)(2,1)} %copy-done.7, ...), custom_call_target="tpu_custom_call" | custom-call | flops 2415919104 | bytes 15000000 | tf_op jit(solution)/shard_map/pallas_call | solution.py:403
  289.4 8.6 %all-to-all-start.1 = ((bf16[32,24,2048]{2,1,0:T(8,128)(2,1)}), bf16[32,24,2048]{2,1,0:T(8,128)(2,1)S(1)}, u32[]{:S(2)}, u32[]{:S(2)}) async-start(bf16[32,24,2048]{2,1,0:T(8,128)(2,1)} %bitcast.55), calls=%async_computation.2 | async-start | bytes 6291456 | tf_op jit(solution)/shard_map/all_to_all | solution.py:589
  298.3 39.6 %all-to-all-done.1 = bf16[32,24,2048]{2,1,0:T(8,128)(2,1)S(1)} async-done(((bf16[32,24,2048]{2,1,0:T(8,128)(2,1)}), bf16[32,24,2048]{2,1,0:T(8,128)(2,1)S(1)}, u32[]{:S(2)}, u32[]{:S(2)}) %all-to-all-start.1) | async-done | bytes 3145760 | tf_op jit(solution)/shard_map/all_to_all | solution.py:589
  337.9 2.3 fusion.7
  340.2 1.1 fusion.52
  341.3 1.9 collective-permute-start.10
  343.2 2.5 fusion.3
  345.6 6.1 %collective-permute-done.10 = bf16[64,2048]{1,0:T(8,128)(2,1)S(1)} collective-permute-done((bf16[64,2048]{1,0:T(8,128)(2,1)S(1)}, bf16[64,2048]{1,0:T(8,128)(2,1)S(1)}, u32[]{:S(2)}, u32[]{:S(2)}) %collective-permute-start.10) | collective-permute-done | bytes 262176 | tf_op jit(solution)/shard_map/ppermute | solution.py:583
  351.8 0.8 pad_maximum_fusion.2
  (95 shorter events, 6.3 us)
Async XLA Ops:
  7.2 20.5 %copy-start.10 = (s32[128,4]{0,1:T(4,128)S(1)}, s32[128,4]{0,1:T(4,128)}, u32[]{:S(2)}) copy-start(s32[128,4]{0,1:T(4,128)} %param.29) | copy-start | bytes 6148
  7.2 22.6 %copy-start.1 = (bf16[128,2048]{1,0:T(8,128)(2,1)S(1)}, bf16[128,2048]{1,0:T(8,128)(2,1)}, u32[]{:S(2)}) copy-start(bf16[128,2048]{1,0:T(8,128)(2,1)} %param.27) | copy-start | bytes 1572868
  7.2 22.9 %copy-start.9 = (f32[2048]{0:T(1024)S(1)}, f32[2048]{0:T(1024)}, u32[]{:S(2)}) copy-start(f32[2048]{0:T(1024)} %param.28) | copy-start | bytes 24580
  7.2 134.7 %all-gather.2.cloned.1.call-start = ((), (), s32[]{:S(2)}) async-start(), calls=%async_computation.3 | async-start | bytes 9732096 | tf_op jit(solution)/shard_map/all_gather | solution.py:481
  7.3 0.9 copy-start.15
  12.8 13.4 %copy-start.2 = (bf16[800,128]{1,0:T(8,128)(2,1)}, bf16[800,128]{1,0:T(8,128)(2,1)S(1)}, u32[]{:S(2)}) copy-start(bf16[800,128]{1,0:T(8,128)(2,1)S(1)} %constant_dynamic-update-slice_fusion) | copy-start | bytes 614404
  12.8 7.8 %collective-permute-start = (bf16[800,128]{1,0:T(8,128)(2,1)S(1)}, bf16[800,128]{1,0:T(8,128)(2,1)S(1)}, u32[]{:S(2)}, u32[]{:S(2)}) collective-permute-start(bf16[800,128]{1,0:T(8,128)(2,1)S(1)} %constant_dynamic-update-slice_fusion), channel_id=1, source_target_pairs={{0,1},{1,2},{2,3},{3,0},{4,5},{5,6},{6,7},{7,4},{8,9},{9,10},{10,1... | collective-permute-start | bytes 614408 | tf_op jit(solution)/shard_map/ppermute | solution.py:475
  14.9 5.7 %collective-permute-start.1 = (bf16[800,128]{1,0:T(8,128)(2,1)S(1)}, bf16[800,128]{1,0:T(8,128)(2,1)S(1)}, u32[]{:S(2)}, u32[]{:S(2)}) collective-permute-start(bf16[800,128]{1,0:T(8,128)(2,1)S(1)} %constant_dynamic-update-slice_fusion), channel_id=1, source_target_pairs={{0,3},{1,0},{2,1},{3,2},{4,7},{5,4},{6,5},{7,6},{8,11},{9,8},{10,9... | collective-permute-start | bytes 614408 | tf_op jit(solution)/shard_map/ppermute | solution.py:476
  16.3 10.0 %collective-permute-start.2 = (bf16[800,128]{1,0:T(8,128)(2,1)S(1)}, bf16[800,128]{1,0:T(8,128)(2,1)S(1)}, u32[]{:S(2)}, u32[]{:S(2)}) collective-permute-start(bf16[800,128]{1,0:T(8,128)(2,1)S(1)} %constant_dynamic-update-slice_fusion), channel_id=1, source_target_pairs={{0,2},{1,3},{2,0},{3,1},{4,6},{5,7},{6,4},{7,5},{8,10},{9,11},{10,... | collective-permute-start | bytes 614408 | tf_op jit(solution)/shard_map/ppermute | solution.py:477
  20.6 5.8 %copy-start.3 = (bf16[800,128]{1,0:T(8,128)(2,1)}, bf16[800,128]{1,0:T(8,128)(2,1)S(1)}, u32[]{:S(2)}) copy-start(bf16[800,128]{1,0:T(8,128)(2,1)S(1)} %collective-permute-done) | copy-start | bytes 614404
  20.6 5.8 %copy-start.4 = (bf16[800,128]{1,0:T(8,128)(2,1)}, bf16[800,128]{1,0:T(8,128)(2,1)S(1)}, u32[]{:S(2)}) copy-start(bf16[800,128]{1,0:T(8,128)(2,1)S(1)} %collective-permute-done.1) | copy-start | bytes 614404
  26.3 0.7 copy-start.5
  30.0 2.9 copy-start.11
  30.0 2.9 copy-start.13
  33.0 64.9 %copy-start.8 = (bf16[256,256]{1,0:T(8,128)(2,1)S(1)}, bf16[256,256]{1,0:T(8,128)(2,1)}, u32[]{:S(2)}) copy-start(bf16[256,256]{1,0:T(8,128)(2,1)} %param.25) | copy-start | bytes 393220
  33.0 87.7 %all-to-all-start = ((bf16[32,24,2048]{2,1,0:T(8,128)(2,1)}), bf16[32,24,2048]{2,1,0:T(8,128)(2,1)S(1)}, u32[]{:S(2)}, u32[]{:S(2)}) async-start(bf16[32,24,2048]{2,1,0:T(8,128)(2,1)} %bitcast.16), calls=%async_computation | async-start | bytes 6291456 | tf_op jit(solution)/shard_map/all_to_all | solution.py:547
  42.7 297.5 %reduce-scatter.2.cloned.1.call-start = ((), (), s32[]{:S(2)}) async-start(), calls=%async_computation.4 | async-start | bytes 2621440 | tf_op jit(solution)/shard_map/reduce_scatter | solution.py:581
  42.8 49.2 %collective-permute-start.4 = (bf16[2048,256]{1,0:T(8,128)(2,1)}, bf16[2048,256]{1,0:T(8,128)(2,1)}, u32[]{:S(2)}, u32[]{:S(2)}) collective-permute-start(bf16[2048,256]{1,0:T(8,128)(2,1)} %bitcast.69), channel_id=1, source_target_pairs={{0,1},{1,2},{2,3},{3,0},{4,5},{5,6},{6,7},{7,4},{8,9},{9,10},{10,1... | collective-permute-start | bytes 3145736 | tf_op jit(solution)/shard_map/ppermute | solution.py:503
  44.8 46.5 %collective-permute-start.3 = (bf16[4,256,128]{2,1,0:T(8,128)(2,1)S(1)}, bf16[4,256,128]{2,1,0:T(8,128)(2,1)}, u32[]{:S(2)}, u32[]{:S(2)}) collective-permute-start(bf16[4,256,128]{2,1,0:T(8,128)(2,1)S(1)} %get-tuple-element.3), channel_id=1, source_target_pairs={{0,124},{1,125},{2,126},{3,127},{4,120},{5,121},{6,122},{7,123},{8... | collective-permute-start | bytes 786440 | tf_op jit(solution)/shard_map/ppermute | solution.py:488
  50.2 54.0 %collective-permute-start.6 = (bf16[256,2048]{1,0:T(8,128)(2,1)}, bf16[256,2048]{1,0:T(8,128)(2,1)}, u32[]{:S(2)}, u32[]{:S(2)}) collective-permute-start(bf16[256,2048]{1,0:T(8,128)(2,1)} %bitcast.75), channel_id=1, source_target_pairs={{0,1},{1,2},{2,3},{3,0},{4,5},{5,6},{6,7},{7,4},{8,9},{9,10},{10,1... | collective-permute-start | bytes 3145736 | tf_op jit(solution)/shard_map/ppermute | solution.py:507
  50.2 56.7 %collective-permute-start.9 = (bf16[256,2048]{1,0:T(8,128)(2,1)}, bf16[256,2048]{1,0:T(8,128)(2,1)}, u32[]{:S(2)}, u32[]{:S(2)}) collective-permute-start(bf16[256,2048]{1,0:T(8,128)(2,1)} %bitcast.76), channel_id=1, source_target_pairs={{0,3},{1,0},{2,1},{3,2},{4,7},{5,4},{6,5},{7,6},{8,11},{9,8},{10,9... | collective-permute-start | bytes 3145736 | tf_op jit(solution)/shard_map/ppermute | solution.py:508
  52.9 51.3 %collective-permute-start.8 = (bf16[2048,256]{1,0:T(8,128)(2,1)}, bf16[2048,256]{1,0:T(8,128)(2,1)}, u32[]{:S(2)}, u32[]{:S(2)}) collective-permute-start(bf16[2048,256]{1,0:T(8,128)(2,1)} %bitcast.72), channel_id=1, source_target_pairs={{0,3},{1,0},{2,1},{3,2},{4,7},{5,4},{6,5},{7,6},{8,11},{9,8},{10,9... | collective-permute-start | bytes 3145736 | tf_op jit(solution)/shard_map/ppermute | solution.py:506
  91.3 25.9 %collective-permute-start.5 = (bf16[2048,256]{1,0:T(8,128)(2,1)}, bf16[2048,256]{1,0:T(8,128)(2,1)}, u32[]{:S(2)}, u32[]{:S(2)}) collective-permute-start(bf16[2048,256]{1,0:T(8,128)(2,1)} %bitcast.73), channel_id=1, source_target_pairs={{0,1},{1,2},{2,3},{3,0},{4,5},{5,6},{6,7},{7,4},{8,9},{9,10},{10,1... | collective-permute-start | bytes 3145736 | tf_op jit(solution)/shard_map/ppermute | solution.py:505
  92.0 28.6 %collective-permute-start.7 = (bf16[2048,256]{1,0:T(8,128)(2,1)}, bf16[2048,256]{1,0:T(8,128)(2,1)}, u32[]{:S(2)}, u32[]{:S(2)}) collective-permute-start(bf16[2048,256]{1,0:T(8,128)(2,1)} %bitcast.70), channel_id=1, source_target_pairs={{0,3},{1,0},{2,1},{3,2},{4,7},{5,4},{6,5},{7,6},{8,11},{9,8},{10,9... | collective-permute-start | bytes 3145736 | tf_op jit(solution)/shard_map/ppermute | solution.py:504
  104.2 173.8 %collective-permute-start.11 = (bf16[2048,256]{1,0:T(8,128)(2,1)}, bf16[2048,256]{1,0:T(8,128)(2,1)}, u32[]{:S(2)}, u32[]{:S(2)}) collective-permute-start(bf16[2048,256]{1,0:T(8,128)(2,1)} %collective-permute-done.4.refs_4_), channel_id=1, source_target_pairs={{0,1},{1,2},{2,3},{3,0},{4,5},{5,6},{6,7},{7,4},{8,9},{9,10},{10,1... | collective-permute-start | bytes 3145736 | tf_op jit(solution)/shard_map/ppermute | solution.py:509
  104.2 173.8 %collective-permute-start.12 = (bf16[2048,256]{1,0:T(8,128)(2,1)}, bf16[2048,256]{1,0:T(8,128)(2,1)}, u32[]{:S(2)}, u32[]{:S(2)}) collective-permute-start(bf16[2048,256]{1,0:T(8,128)(2,1)} %collective-permute-done.8.refs_8_), channel_id=1, source_target_pairs={{0,3},{1,0},{2,1},{3,2},{4,7},{5,4},{6,5},{7,6},{8,11},{9,8},{10,9... | collective-permute-start | bytes 3145736 | tf_op jit(solution)/shard_map/ppermute | solution.py:510
  120.7 1.7 copy-start
  254.0 17.9 %collective-permute-start.13 = (bf16[128,2048]{1,0:T(8,128)(2,1)S(1)}, bf16[128,2048]{1,0:T(8,128)(2,1)S(1)}, u32[]{:S(2)}, u32[]{:S(2)}) collective-permute-start(bf16[128,2048]{1,0:T(8,128)(2,1)S(1)} %slice.166), channel_id=1, source_target_pairs={{0,1},{1,2},{2,3},{3,0},{4,5},{5,6},{6,7},{7,4},{8,9},{9,10},{10,1... | collective-permute-start | bytes 1572872 | tf_op jit(solution)/shard_map/ppermute | solution.py:512
  256.4 21.6 %collective-permute-start.14 = (bf16[128,2048]{1,0:T(8,128)(2,1)S(1)}, bf16[128,2048]{1,0:T(8,128)(2,1)S(1)}, u32[]{:S(2)}, u32[]{:S(2)}) collective-permute-start(bf16[128,2048]{1,0:T(8,128)(2,1)S(1)} %slice.167), channel_id=1, source_target_pairs={{0,3},{1,0},{2,1},{3,2},{4,7},{5,4},{6,5},{7,6},{8,11},{9,8},{10,9... | collective-permute-start | bytes 1572872 | tf_op jit(solution)/shard_map/ppermute | solution.py:513
  271.9 6.1 %copy-start.6 = (bf16[128,2048]{1,0:T(8,128)(2,1)}, bf16[128,2048]{1,0:T(8,128)(2,1)S(1)}, u32[]{:S(2)}) copy-start(bf16[128,2048]{1,0:T(8,128)(2,1)S(1)} %collective-permute-done.13.refs_3_) | copy-start | bytes 1572868
  278.0 0.8 copy-start.7
  289.3 8.7 %copy-start.16 = (f32[128,4]{0,1:T(4,128)S(1)}, f32[128,4]{0,1:T(4,128)}, u32[]{:S(2)}) copy-start(f32[128,4]{0,1:T(4,128)} %param.30) | copy-start | bytes 6148
  289.3 8.7 %copy-start.12 = (s32[128]{0:T(128)S(1)}, s32[128]{0:T(128)}, u32[]{:S(2)}) copy-start(s32[128]{0:T(128)} %copy-done.11) | copy-start | bytes 1540
  289.3 8.7 %copy-start.14 = (s32[128]{0:T(128)S(1)}, s32[128]{0:T(128)}, u32[]{:S(2)}) copy-start(s32[128]{0:T(128)} %copy-done.13) | copy-start | bytes 1540
  289.4 48.5 %all-to-all-start.1 = ((bf16[32,24,2048]{2,1,0:T(8,128)(2,1)}), bf16[32,24,2048]{2,1,0:T(8,128)(2,1)S(1)}, u32[]{:S(2)}, u32[]{:S(2)}) async-start(bf16[32,24,2048]{2,1,0:T(8,128)(2,1)} %bitcast.55), calls=%async_computation.2 | async-start | bytes 6291456 | tf_op jit(solution)/shard_map/all_to_all | solution.py:589
  341.3 10.5 %collective-permute-start.10 = (bf16[64,2048]{1,0:T(8,128)(2,1)S(1)}, bf16[64,2048]{1,0:T(8,128)(2,1)S(1)}, u32[]{:S(2)}, u32[]{:S(2)}) collective-permute-start(bf16[64,2048]{1,0:T(8,128)(2,1)S(1)} %get-tuple-element.5), channel_id=1, source_target_pairs={{0,124},{1,125},{2,126},{3,127},{4,120},{5,121},{6,122},{7,123},{8... | collective-permute-start | bytes 786440 | tf_op jit(solution)/shard_map/ppermute | solution.py:583
Sparse Core Ops, SparseCore 0:
  27.8 92.0 all-gather.1
  253.1 35.2 reduce-scatter.1

commit v2 on v1

--- a/solution.py
+++ b/solution.py
@@ -320,6 +320,7 @@
 
 ROWS = 256
 COLUMNS = 512
+IN_FLIGHT = 4
 
 
 def experts_kernel(pieces, carried, x_ref, *refs):
@@ -346,11 +347,13 @@
                 n += 1
             copies.append(own)
     first_step = pl.program_id(0) == 0
+    turn = [n for b in range(len(pieces)) for n in (3 * b, 3 * b + 1)]
+    turn = turn + [3 * b + 2 for b in range(len(pieces))]
 
     @pl.when(first_step)
     def _():
-        for own in copies:
-            for copy in own:
+        for n in turn[:IN_FLIGHT]:
+            for copy in copies[n]:
                 copy.start()
 
     def ready(n):
@@ -358,6 +361,10 @@
         def _():
             for copy in copies[n]:
                 copy.wait()
+            later = turn.index(n) + IN_FLIGHT
+            if later < len(turn):
+                for copy in copies[turn[later]]:
+                    copy.start()
 
     rows = x_ref[...]
     hidden = []
@@ -468,25 +475,30 @@
         for half in range(2)
         for n in range(4)
     ]
-    own = jnp.concatenate([kv_normed[:, :128], kv_normed[:, 128:], k_packed, *q_packed], axis=0)
-    group = jnp.stack(
-        [
-            own,
-            lax.ppermute(own, both, shift(1)),
-            lax.ppermute(own, both, shift(-1)),
-            lax.ppermute(own, both, shift(2)),
-        ]
-    )
-    kv_rows = 2 * tok_rows + 32
-    kv_all = lax.all_gather(group[:, :kv_rows], "ep", axis=0, tiled=True)
+    kv_own = jnp.concatenate([kv_normed[:, :128], kv_normed[:, 128:], k_packed], axis=0)
+    q_own = jnp.concatenate(q_packed, axis=0)
+
+    def with_neighbours(own):
+        return jnp.stack(
+            [
+                own,
+                lax.ppermute(own, both, shift(1)),
+                lax.ppermute(own, both, shift(-1)),
+                lax.ppermute(own, both, shift(2)),
+            ]
+        )
+
+    kv_near = with_neighbours(kv_own)
+    q_near = with_neighbours(q_own)
+    kv_all = lax.all_gather(kv_near, "ep", axis=0, tiled=True)
     behind = (jnp.arange(tp_count, dtype=jnp.int32) - tp) % tp_count
     order = jnp.where(behind == 0, 0, jnp.where(behind == 3, 1, jnp.where(behind == 1, 2, 3)))
     place = jnp.concatenate(
         [jnp.stack([ep, jnp.maximum(ep, ep_count - 1 - ep)]), order]
     ).astype(jnp.int32)
 
-    q_mirrored = lax.ppermute(group[:, kv_rows + tok_rows * 2 :], both, mirror)
-    q_both = jnp.stack([group[:, kv_rows : kv_rows + tok_rows * 2], q_mirrored])
+    q_mirrored = lax.ppermute(q_near[:, tok_rows * 2 :], both, mirror)
+    q_both = jnp.stack([q_near[:, : tok_rows * 2], q_mirrored])
     spread = (
         jnp.arange(tp_count, dtype=jnp.int32)[:, None] * tok_rows
         + jnp.arange(half_rows, dtype=jnp.int32)[None, :]
@@ -499,19 +511,15 @@
     q_sine = q_sine.reshape(2, QUERIES, ROPE // 2).transpose(0, 2, 1)
 
     gate, up, down = w_gate_exp[0], w_up_exp[0], w_down_exp[0]
-    half_units = down.shape[0] // 2
     gate_left = lax.ppermute(gate, both, shift(1))
     gate_right = lax.ppermute(gate, both, shift(-1))
     up_left = lax.ppermute(up, both, shift(1))
     up_right = lax.ppermute(up, both, shift(-1))
     down_left = lax.ppermute(down, both, shift(1))
     down_right = lax.ppermute(down, both, shift(-1))
+    down_across = lax.ppermute(down, both, shift(2))
     gate_across = lax.ppermute(gate_left, both, shift(1))
-    up_across = lax.ppermute(up_right, both, shift(-1))
-    down_across = [
-        lax.ppermute(down_left[:half_units], both, shift(1)),
-        lax.ppermute(down_right[half_units:], both, shift(-1)),
-    ]
+    up_across = lax.ppermute(up_left, both, shift(1))
 
     expert_count = ep_count
     slot_count = 3 * tok_rows * TOPK // (2 * expert_count)
@@ -553,18 +561,6 @@
     )
     chosen = arrived.reshape(expert_count * slot_count, D)
 
-    near = experts(
-        chosen,
-        [
-            ([gate], [up], [down]),
-            ([gate_left], [up_left], [down_left]),
-            ([gate_right], [up_right], [down_right]),
-        ],
-        None,
-        place,
-        jnp.float32,
-    )
-
     partial_out = attention(
         place,
         kv_all,
@@ -576,7 +572,7 @@
         w_key,
         w_value.T,
         w_mix_out,
-        near,
+        place,
     ).reshape(group_rows, D)
     mixed = lax.psum_scatter(partial_out, "tp", scatter_dimension=0, tiled=True)
     mixer_out = jnp.concatenate(
@@ -584,7 +580,16 @@
     )
 
     results = experts(
-        chosen, [([gate_across], [up_across], down_across)], near, partial_out, jnp.bfloat16
+        chosen,
+        [
+            ([gate], [up], [down]),
+            ([gate_left], [up_left], [down_left]),
+            ([gate_right], [up_right], [down_right]),
+            ([gate_across], [up_across], [down_across]),
+        ],
+        None,
+        partial_out,
+        jnp.bfloat16,
     )
     returned = lax.all_to_all(
         results.reshape(expert_count, slot_count, D),

time: 362 us -> 321 us (0.89)
  waiting for transfers between devices: 125 us -> 94.9 us
  Pallas kernels: 141 us -> 136 us
    ppermute x7 -> x9, waiting for transfers between devices: 65.5 us -> 49.1 us  [the longest x1 46.1 us: layer(): q_mirrored = lax.ppermute(q_near[:, tok_rows * 2:], both, mirror)]
    ppermute x1, waiting for transfers between devices: 10.2 us -> 0.01 us  [layer(): up_left = lax.ppermute(up, both, shift(1))]
    pallas_call x2 -> x1, Pallas kernels: 30 us -> 24.8 us  [experts(): pl.pallas_call(body, grid=(rows.shape[0] // ROWS,), in_specs=in_specs, ou...]
    ppermute x7 -> x9, starting transfers between devices: 16.7 us -> 15 us  [the longest x1 5.6 us: layer(): q_mirrored = lax.ppermute(q_near[:, tok_rows * 2:], both, mirror)]
    unnamed x51 -> x37, local copies, waits for them, and re-layouts: 7.79 us -> 7.13 us
  transfers between devices with their start and end apart: 19 -> 21, of which waited for: 9 -> 5; matrix products, arithmetic and copies ran while one was open for 7% -> 8% of each run, Pallas kernels for 39% -> 43%
where the time goes in v2:
time: 321 us; the launch traced here: 319 us
  Pallas kernels  136 us (42%)
  waiting for transfers between devices  94.9 us (30%)
  starting transfers between devices  40.6 us (13%)
  other arithmetic  16.5 us (5%)
  between operations  14.5 us (5%)
  local copies, waits for them, and re-layouts  10.9 us (3%)
  matrix products  5.21 us (2%)
    pallas_call x1, Pallas kernels, attention(): pl.pallas_call(attention_kernel, in_specs=[pl.BlockSpec(memory_space=pltp...  111 us
    ppermute x1, waiting for transfers between devices, layer(): q_mirrored = lax.ppermute(q_near[:, tok_rows * 2:], both, mirror)  46.1 us
    all_to_all x1, waiting for transfers between devices, layer(): lax.all_to_all(results.reshape(expert_count, slot_count, D), 'ep', split_...  39.6 us
    pallas_call x1, Pallas kernels, experts(): pl.pallas_call(body, grid=(rows.shape[0] // ROWS,), in_specs=in_specs, ou...  24.8 us
    all_to_all x1, starting transfers between devices, layer(): lax.all_to_all(outgoing.reshape(expert_count, slot_count, D), 'ep', split...  12 us
    unnamed x37, local copies, waits for them, and re-layouts  7.13 us
  transfers between devices with their start and end apart: 21, of which 5 were waited for; matrix products, arithmetic and copies ran while one was open for 8% of the time, Pallas kernels for 43%

profile of v2, /device:TPU:1, one launch (start us, length us, event | category | flops | bytes accessed | tf_op | source)
XLA Modules:
  0.0 318.6 jit_solution(15869423331571918248)
XLA Ops:
  7.3 0.8 convert_element_type.73
  8.6 1.0 fusion.30
  9.6 0.9 fusion.32
  10.6 2.1 collective-permute-start
  12.7 1.3 collective-permute-start.1
  14.0 1.6 collective-permute-start.2
  15.9 2.9 collective-permute-done.2
  18.8 0.8 pad_maximum_fusion.3
  19.6 1.0 fusion.16
  20.6 1.0 fusion.18
  21.7 0.6 collective-permute-start.3
  22.4 2.1 collective-permute-start.4
  24.5 0.4 collective-permute-start.5
  24.9 0.8 collective-permute-start.10
  25.6 1.9 collective-permute-start.13
  27.6 0.8 copy.60
  28.6 1.2 reduce-window.6
  30.6 2.9 convolution_convert_fusion
  33.5 12.0 %all-to-all-start = ((bf16[32,24,2048]{2,1,0:T(8,128)(2,1)}), bf16[32,24,2048]{2,1,0:T(8,128)(2,1)S(1)}, u32[]{:S(2)}, u32[]{:S(2)}) async-start(bf16[32,24,2048]{2,1,0:T(8,128)(2,1)} %bitcast.25), calls=%async_computation.1 | async-start | bytes 6291456 | tf_op jit(solution)/shard_map/all_to_all | solution.py:555
  45.7 1.1 collective-permute-start.9
  46.8 0.7 add.149
  47.5 0.6 add.153
  48.1 0.7 fusion.47
  48.9 1.0 pad_maximum_fusion
  49.9 0.7 slice_bitcast_fusion
  50.6 5.6 %collective-permute-start.6 = (bf16[4,256,128]{2,1,0:T(8,128)(2,1)}, bf16[4,256,128]{2,1,0:T(8,128)(2,1)}, u32[]{:S(2)}, u32[]{:S(2)}) collective-permute-start(bf16[4,256,128]{2,1,0:T(8,128)(2,1)} %get-tuple-element.5), channel_id=1, source_target_pairs={{0,124},{1,125},{2,126},{3,127},{4,120},{5,121},{6,122},{7,123},{8... | collective-permute-start | bytes 786440 | tf_op jit(solution)/shard_map/ppermute | solution.py:500
  56.2 1.4 multiply_sine_fusion
  57.7 1.8 copy.57
  59.4 0.8 copy.58
  60.2 1.7 copy.59
  61.9 0.6 pad_add_fusion.place_ref.after_ref
  62.5 46.1 %collective-permute-done.6 = bf16[4,256,128]{2,1,0:T(8,128)(2,1)} collective-permute-done((bf16[4,256,128]{2,1,0:T(8,128)(2,1)}, bf16[4,256,128]{2,1,0:T(8,128)(2,1)}, u32[]{:S(2)}, u32[]{:S(2)}) %collective-permute-start.6) | collective-permute-done | bytes 262176 | tf_op jit(solution)/shard_map/ppermute | solution.py:500
  108.6 0.8 collective-permute-start.16
  109.3 1.8 pad_maximum_fusion.1.q_ref
  111.1 0.3 collective-permute-start.11
  111.5 2.2 collective-permute-start.12
  113.6 0.4 collective-permute-start.15
  114.1 111.2 %attention.1 = bf16[4,2,64,2048]{3,2,1,0:T(8,128)(2,1)} custom-call(s32[6]{0:T(128)} %pad_add_fusion.place_ref.after_ref, bf16[128,288,128]{2,1,0:T(8,128)(2,1)} %all-gather.2.cloned.1.call-done.kv_ref, bf16[2,4,256,128]{3,2,1,0:T(8,128)(2,1)} %pad_maximum_fusion.1.q_ref, bf16[256,512]{1,0:T(8,128)(2,1)} %bitcast.62, bf16[128,512]{1,0:T(8,128)(2,1)} %bitcast.64, ...), custom_call_target="tpu_custom_call" | custom-call | flops 30000001024 | bytes 16000000 | tf_op jit(solution)/shard_map/attention/pallas_call | solution.py:294
  225.4 1.7 copy-done
  227.1 24.8 %shard_map.176 = bf16[768,2048]{1,0:T(8,128)(2,1)} custom-call(bf16[768,2048]{1,0:T(8,128)(2,1)} %bitcast.58, bf16[2048,256]{1,0:T(8,128)(2,1)} %bitcast.72, bf16[2048,256]{1,0:T(8,128)(2,1)} %bitcast.75, bf16[256,2048]{1,0:T(8,128)(2,1)} %bitcast.79, bf16[2048,256]{1,0:T(8,128)(2,1)} %collective-permute-done.8.refs_4_, ...), custom_call_target="tpu_custom_call" | custom-call | flops 9663676416 | bytes 24000000 | tf_op jit(solution)/shard_map/pallas_call | solution.py:410
  251.9 5.2 %all-to-all-start.1 = ((bf16[32,24,2048]{2,1,0:T(8,128)(2,1)}), bf16[32,24,2048]{2,1,0:T(8,128)(2,1)S(1)}, u32[]{:S(2)}, u32[]{:S(2)}) async-start(bf16[32,24,2048]{2,1,0:T(8,128)(2,1)} %bitcast.59), calls=%async_computation.2 | async-start | bytes 6291456 | tf_op jit(solution)/shard_map/all_to_all | solution.py:594
  257.5 39.6 %all-to-all-done.1 = bf16[32,24,2048]{2,1,0:T(8,128)(2,1)S(1)} async-done(((bf16[32,24,2048]{2,1,0:T(8,128)(2,1)}), bf16[32,24,2048]{2,1,0:T(8,128)(2,1)S(1)}, u32[]{:S(2)}, u32[]{:S(2)}) %all-to-all-start.1) | async-done | bytes 3145760 | tf_op jit(solution)/shard_map/all_to_all | solution.py:594
  297.1 2.3 fusion.7
  299.4 1.1 fusion.52
  300.4 1.9 collective-permute-start.7
  302.4 2.5 fusion.3
  304.8 6.1 %collective-permute-done.7 = bf16[64,2048]{1,0:T(8,128)(2,1)S(1)} collective-permute-done((bf16[64,2048]{1,0:T(8,128)(2,1)S(1)}, bf16[64,2048]{1,0:T(8,128)(2,1)S(1)}, u32[]{:S(2)}, u32[]{:S(2)}) %collective-permute-start.7) | collective-permute-done | bytes 262176 | tf_op jit(solution)/shard_map/ppermute | solution.py:579
  311.0 0.8 pad_maximum_fusion.2
  (84 shorter events, 2.6 us)
Async XLA Ops:
  7.2 23.3 %copy-start.4 = (s32[128,4]{0,1:T(4,128)S(1)}, s32[128,4]{0,1:T(4,128)}, u32[]{:S(2)}) copy-start(s32[128,4]{0,1:T(4,128)} %param.29) | copy-start | bytes 6148
  7.2 23.1 %copy-start.1 = (bf16[128,2048]{1,0:T(8,128)(2,1)S(1)}, bf16[128,2048]{1,0:T(8,128)(2,1)}, u32[]{:S(2)}) copy-start(bf16[128,2048]{1,0:T(8,128)(2,1)} %param.27) | copy-start | bytes 1572868
  7.2 23.4 %copy-start.3 = (f32[2048]{0:T(1024)S(1)}, f32[2048]{0:T(1024)}, u32[]{:S(2)}) copy-start(f32[2048]{0:T(1024)} %param.28) | copy-start | bytes 24580
  7.2 106.9 %all-gather.2.cloned.1.call-start = ((), (), s32[]{:S(2)}) async-start(), calls=%async_computation.3 | async-start | bytes 9732096 | tf_op jit(solution)/shard_map/all_gather | solution.py:493
  7.3 0.9 copy-start.9
  10.6 5.2 %collective-permute-start = (bf16[288,128]{1,0:T(8,128)(2,1)S(1)}, bf16[288,128]{1,0:T(8,128)(2,1)S(1)}, u32[]{:S(2)}, u32[]{:S(2)}) collective-permute-start(bf16[288,128]{1,0:T(8,128)(2,1)S(1)} %maximum_maximum_fusion), channel_id=1, source_target_pairs={{0,1},{1,2},{2,3},{3,0},{4,5},{5,6},{6,7},{7,4},{8,9},{9,10},{10,1... | collective-permute-start | bytes 221192 | tf_op jit(solution)/shard_map/ppermute | solution.py:485
  12.7 3.2 %collective-permute-start.1 = (bf16[288,128]{1,0:T(8,128)(2,1)S(1)}, bf16[288,128]{1,0:T(8,128)(2,1)S(1)}, u32[]{:S(2)}, u32[]{:S(2)}) collective-permute-start(bf16[288,128]{1,0:T(8,128)(2,1)S(1)} %maximum_maximum_fusion), channel_id=1, source_target_pairs={{0,3},{1,0},{2,1},{3,2},{4,7},{5,4},{6,5},{7,6},{8,11},{9,8},{10,9... | collective-permute-start | bytes 221192 | tf_op jit(solution)/shard_map/ppermute | solution.py:486
  14.0 4.8 %collective-permute-start.2 = (bf16[288,128]{1,0:T(8,128)(2,1)S(1)}, bf16[288,128]{1,0:T(8,128)(2,1)S(1)}, u32[]{:S(2)}, u32[]{:S(2)}) collective-permute-start(bf16[288,128]{1,0:T(8,128)(2,1)S(1)} %maximum_maximum_fusion), channel_id=1, source_target_pairs={{0,2},{1,3},{2,0},{3,1},{4,6},{5,7},{6,4},{7,5},{8,10},{9,11},{10,... | collective-permute-start | bytes 221192 | tf_op jit(solution)/shard_map/ppermute | solution.py:487
  21.7 23.8 %collective-permute-start.3 = (bf16[512,128]{1,0:T(8,128)(2,1)S(1)}, bf16[512,128]{1,0:T(8,128)(2,1)S(1)}, u32[]{:S(2)}, u32[]{:S(2)}) collective-permute-start(bf16[512,128]{1,0:T(8,128)(2,1)S(1)} %constant_dynamic-update-slice_fusion), channel_id=1, source_target_pairs={{0,1},{1,2},{2,3},{3,0},{4,5},{5,6},{6,7},{7,4},{8,9},{9,10},{10,1... | collective-permute-start | bytes 393224 | tf_op jit(solution)/shard_map/ppermute | solution.py:485
  22.4 23.3 %collective-permute-start.4 = (bf16[512,128]{1,0:T(8,128)(2,1)S(1)}, bf16[512,128]{1,0:T(8,128)(2,1)}, u32[]{:S(2)}, u32[]{:S(2)}) collective-permute-start(bf16[512,128]{1,0:T(8,128)(2,1)S(1)} %constant_dynamic-update-slice_fusion), channel_id=1, source_target_pairs={{0,3},{1,0},{2,1},{3,2},{4,7},{5,4},{6,5},{7,6},{8,11},{9,8},{10,9... | collective-permute-start | bytes 393224 | tf_op jit(solution)/shard_map/ppermute | solution.py:486
  24.5 24.4 %collective-permute-start.5 = (bf16[512,128]{1,0:T(8,128)(2,1)S(1)}, bf16[512,128]{1,0:T(8,128)(2,1)}, u32[]{:S(2)}, u32[]{:S(2)}) collective-permute-start(bf16[512,128]{1,0:T(8,128)(2,1)S(1)} %constant_dynamic-update-slice_fusion), channel_id=1, source_target_pairs={{0,2},{1,3},{2,0},{3,1},{4,6},{5,7},{6,4},{7,5},{8,10},{9,11},{10,... | collective-permute-start | bytes 393224 | tf_op jit(solution)/shard_map/ppermute | solution.py:487
  24.9 88.8 %collective-permute-start.10 = (bf16[256,2048]{1,0:T(8,128)(2,1)}, bf16[256,2048]{1,0:T(8,128)(2,1)}, u32[]{:S(2)}, u32[]{:S(2)}) collective-permute-start(bf16[256,2048]{1,0:T(8,128)(2,1)} %bitcast.76), channel_id=1, source_target_pairs={{0,1},{1,2},{2,3},{3,0},{4,5},{5,6},{6,7},{7,4},{8,9},{9,10},{10,1... | collective-permute-start | bytes 3145736 | tf_op jit(solution)/shard_map/ppermute | solution.py:518
  25.6 88.0 %collective-permute-start.13 = (bf16[256,2048]{1,0:T(8,128)(2,1)}, bf16[256,2048]{1,0:T(8,128)(2,1)}, u32[]{:S(2)}, u32[]{:S(2)}) collective-permute-start(bf16[256,2048]{1,0:T(8,128)(2,1)} %bitcast.77), channel_id=1, source_target_pairs={{0,3},{1,0},{2,1},{3,2},{4,7},{5,4},{6,5},{7,6},{8,11},{9,8},{10,9... | collective-permute-start | bytes 3145736 | tf_op jit(solution)/shard_map/ppermute | solution.py:519
  30.5 2.9 copy-start.5
  30.6 2.9 copy-start.7
  33.5 26.0 %copy-start.2 = (bf16[512,128]{1,0:T(8,128)(2,1)S(1)}, bf16[512,128]{1,0:T(8,128)(2,1)}, u32[]{:S(2)}) copy-start(bf16[512,128]{1,0:T(8,128)(2,1)} %param.23) | copy-start | bytes 393220
  33.5 191.9 %all-to-all-start = ((bf16[32,24,2048]{2,1,0:T(8,128)(2,1)}), bf16[32,24,2048]{2,1,0:T(8,128)(2,1)S(1)}, u32[]{:S(2)}, u32[]{:S(2)}) async-start(bf16[32,24,2048]{2,1,0:T(8,128)(2,1)} %bitcast.25), calls=%async_computation.1 | async-start | bytes 6291456 | tf_op jit(solution)/shard_map/all_to_all | solution.py:555
  45.5 253.9 %reduce-scatter.2.cloned.1.call-start = ((), (), s32[]{:S(2)}) async-start(), calls=%async_computation.4 | async-start | bytes 2621440 | tf_op jit(solution)/shard_map/reduce_scatter | solution.py:577
  45.6 65.6 %collective-permute-start.8 = (bf16[2048,256]{1,0:T(8,128)(2,1)}, bf16[2048,256]{1,0:T(8,128)(2,1)}, u32[]{:S(2)}, u32[]{:S(2)}) collective-permute-start(bf16[2048,256]{1,0:T(8,128)(2,1)} %bitcast.70), channel_id=1, source_target_pairs={{0,1},{1,2},{2,3},{3,0},{4,5},{5,6},{6,7},{7,4},{8,9},{9,10},{10,1... | collective-permute-start | bytes 3145736 | tf_op jit(solution)/shard_map/ppermute | solution.py:514
  45.7 65.8 %collective-permute-start.9 = (bf16[2048,256]{1,0:T(8,128)(2,1)}, bf16[2048,256]{1,0:T(8,128)(2,1)}, u32[]{:S(2)}, u32[]{:S(2)}) collective-permute-start(bf16[2048,256]{1,0:T(8,128)(2,1)} %bitcast.73), channel_id=1, source_target_pairs={{0,1},{1,2},{2,3},{3,0},{4,5},{5,6},{6,7},{7,4},{8,9},{9,10},{10,1... | collective-permute-start | bytes 3145736 | tf_op jit(solution)/shard_map/ppermute | solution.py:516
  50.6 57.9 %collective-permute-start.6 = (bf16[4,256,128]{2,1,0:T(8,128)(2,1)}, bf16[4,256,128]{2,1,0:T(8,128)(2,1)}, u32[]{:S(2)}, u32[]{:S(2)}) collective-permute-start(bf16[4,256,128]{2,1,0:T(8,128)(2,1)} %get-tuple-element.5), channel_id=1, source_target_pairs={{0,124},{1,125},{2,126},{3,127},{4,120},{5,121},{6,122},{7,123},{8... | collective-permute-start | bytes 786440 | tf_op jit(solution)/shard_map/ppermute | solution.py:500
  108.6 116.8 %collective-permute-start.16 = (bf16[256,2048]{1,0:T(8,128)(2,1)}, bf16[256,2048]{1,0:T(8,128)(2,1)}, u32[]{:S(2)}, u32[]{:S(2)}) collective-permute-start(bf16[256,2048]{1,0:T(8,128)(2,1)} %bitcast.78), channel_id=1, source_target_pairs={{0,2},{1,3},{2,0},{3,1},{4,6},{5,7},{6,4},{7,5},{8,10},{9,11},{10,... | collective-permute-start | bytes 3145736 | tf_op jit(solution)/shard_map/ppermute | solution.py:520
  111.1 114.2 %collective-permute-start.11 = (bf16[2048,256]{1,0:T(8,128)(2,1)}, bf16[2048,256]{1,0:T(8,128)(2,1)}, u32[]{:S(2)}, u32[]{:S(2)}) collective-permute-start(bf16[2048,256]{1,0:T(8,128)(2,1)} %bitcast.71), channel_id=1, source_target_pairs={{0,3},{1,0},{2,1},{3,2},{4,7},{5,4},{6,5},{7,6},{8,11},{9,8},{10,9... | collective-permute-start | bytes 3145736 | tf_op jit(solution)/shard_map/ppermute | solution.py:515
  111.5 113.9 %collective-permute-start.12 = (bf16[2048,256]{1,0:T(8,128)(2,1)}, bf16[2048,256]{1,0:T(8,128)(2,1)}, u32[]{:S(2)}, u32[]{:S(2)}) collective-permute-start(bf16[2048,256]{1,0:T(8,128)(2,1)} %bitcast.74), channel_id=1, source_target_pairs={{0,3},{1,0},{2,1},{3,2},{4,7},{5,4},{6,5},{7,6},{8,11},{9,8},{10,9... | collective-permute-start | bytes 3145736 | tf_op jit(solution)/shard_map/ppermute | solution.py:517
  113.6 111.7 %collective-permute-start.14 = (bf16[2048,256]{1,0:T(8,128)(2,1)}, bf16[2048,256]{1,0:T(8,128)(2,1)}, u32[]{:S(2)}, u32[]{:S(2)}) collective-permute-start(bf16[2048,256]{1,0:T(8,128)(2,1)} %collective-permute-done.8.refs_4_), channel_id=1, source_target_pairs={{0,1},{1,2},{2,3},{3,0},{4,5},{5,6},{6,7},{7,4},{8,9},{9,10},{10,1... | collective-permute-start | bytes 3145736 | tf_op jit(solution)/shard_map/ppermute | solution.py:521
  113.6 111.7 %collective-permute-start.15 = (bf16[2048,256]{1,0:T(8,128)(2,1)}, bf16[2048,256]{1,0:T(8,128)(2,1)}, u32[]{:S(2)}, u32[]{:S(2)}) collective-permute-start(bf16[2048,256]{1,0:T(8,128)(2,1)} %collective-permute-done.9.refs_5_), channel_id=1, source_target_pairs={{0,1},{1,2},{2,3},{3,0},{4,5},{5,6},{6,7},{7,4},{8,9},{9,10},{10,1... | collective-permute-start | bytes 3145736 | tf_op jit(solution)/shard_map/ppermute | solution.py:522
  225.4 1.7 copy-start
  251.9 5.3 %copy-start.10 = (f32[128,4]{0,1:T(4,128)S(1)}, f32[128,4]{0,1:T(4,128)}, u32[]{:S(2)}) copy-start(f32[128,4]{0,1:T(4,128)} %param.30) | copy-start | bytes 6148
  251.9 5.3 %copy-start.6 = (s32[128]{0:T(128)S(1)}, s32[128]{0:T(128)}, u32[]{:S(2)}) copy-start(s32[128]{0:T(128)} %copy-done.5) | copy-start | bytes 1540
  251.9 5.3 %copy-start.8 = (s32[128]{0:T(128)S(1)}, s32[128]{0:T(128)}, u32[]{:S(2)}) copy-start(s32[128]{0:T(128)} %copy-done.7) | copy-start | bytes 1540
  251.9 45.1 %all-to-all-start.1 = ((bf16[32,24,2048]{2,1,0:T(8,128)(2,1)}), bf16[32,24,2048]{2,1,0:T(8,128)(2,1)S(1)}, u32[]{:S(2)}, u32[]{:S(2)}) async-start(bf16[32,24,2048]{2,1,0:T(8,128)(2,1)} %bitcast.59), calls=%async_computation.2 | async-start | bytes 6291456 | tf_op jit(solution)/shard_map/all_to_all | solution.py:594
  300.4 10.5 %collective-permute-start.7 = (bf16[64,2048]{1,0:T(8,128)(2,1)S(1)}, bf16[64,2048]{1,0:T(8,128)(2,1)S(1)}, u32[]{:S(2)}, u32[]{:S(2)}) collective-permute-start(bf16[64,2048]{1,0:T(8,128)(2,1)S(1)} %get-tuple-element.3), channel_id=1, source_target_pairs={{0,124},{1,125},{2,126},{3,127},{4,120},{5,121},{6,122},{7,123},{8... | collective-permute-start | bytes 786440 | tf_op jit(solution)/shard_map/ppermute | solution.py:579
Sparse Core Ops, SparseCore 0:
  19.7 89.7 all-gather.1
  225.5 27.4 reduce-scatter.1

commit v3 on v2

--- a/solution.py
+++ b/solution.py
@@ -22,7 +22,7 @@
 QUERIES = 256
 HEADS_HERE = 4
 STEPS_A_CHUNK = 4
-PIECE = 256
+PIECE = 128
 excess_limit = 60.0
 exponent_scale = (NOPE + ROPE) ** (-0.5) * math.log2(math.e)
 
@@ -118,8 +118,9 @@
             query_ref[half, h, 128:144] = (first * cosine - second * sine).astype(jnp.bfloat16)
             query_ref[half, h, 144:160] = (first * sine + second * cosine).astype(jnp.bfloat16)
             query_ref[half, h, 160:256] = jnp.zeros((96, QUERIES), jnp.bfloat16)
-    for h in range(HEADS_HERE):
-        vt_ref[h, 64:80] = jnp.ones((16, KEYS), jnp.bfloat16)
+    for slot in range(2):
+        for h in range(HEADS_HERE):
+            vt_ref[slot, h, 64:80] = jnp.ones((16, KEYS), jnp.bfloat16)
 
     def clear():
         max_ref[...] = jnp.full_like(max_ref, masked_score)
@@ -144,11 +145,16 @@
         vals = lax.dot_general(
             wv_ref[...], normed, BY_LAST, preferred_element_type=jnp.float32
         ).astype(jnp.bfloat16)
-        for p in range(2):
-            pair_ref[p, :, 0:128] = keys[:, p * 128 : p * 128 + 128]
-            pair_ref[p, :, 128:256] = rope
-        for h in range(HEADS_HERE):
-            vt_ref[h, 0:64] = vals[h * 64 : h * 64 + 64]
+
+        def store():
+            slot = j % 2
+            for p in range(2):
+                pair_ref[slot, p, :, 0:128] = keys[:, p * 128 : p * 128 + 128]
+                pair_ref[slot, p, :, 128:256] = rope
+            for h in range(HEADS_HERE):
+                vt_ref[slot, h, 0:64] = vals[h * 64 : h * 64 + 64]
+
+        return store
 
     def hidden_keys(j, half):
         edge = jnp.where(half == 0, group, 31 - group)
@@ -162,14 +168,14 @@
         hidden = hidden_keys(j, half)
         for h in range(HEADS_HERE):
             scores = jnp.dot(
-                pair_ref[h // 2], query_ref[half, h], preferred_element_type=jnp.float32
+                pair_ref[j % 2, h // 2], query_ref[half, h], preferred_element_type=jnp.float32
             )
             scores = jnp.where(hidden, masked_score, scores)
             old = max_ref[half, h, 0:1]
             new = jnp.maximum(old, jnp.max(scores, axis=0, keepdims=True))
             factor = jnp.exp2((old - new) * exponent_scale)
             weights = jnp.exp2((scores - new) * exponent_scale).astype(jnp.bfloat16)
-            part = jnp.dot(vt_ref[h], weights, preferred_element_type=jnp.float32)
+            part = jnp.dot(vt_ref[j % 2, h], weights, preferred_element_type=jnp.float32)
             sum_ref[half, h] = sum_ref[half, h] * factor + part
             max_ref[half, h, 0:1] = new
 
@@ -185,7 +191,7 @@
             tops, pieces = [], []
             for p in range(0, KEYS, PIECE):
                 scores = jnp.dot(
-                    pair_ref[h // 2, p : p + PIECE],
+                    pair_ref[j % 2, h // 2, p : p + PIECE],
                     query_ref[half, h],
                     preferred_element_type=jnp.float32,
                 )
@@ -203,30 +209,35 @@
 
         def gather(u):
             half, h = units[u]
-            part = jnp.dot(vt_ref[h], weights[u], preferred_element_type=jnp.float32)
+            part = jnp.dot(vt_ref[j % 2, h], weights[u], preferred_element_type=jnp.float32)
             new = jnp.maximum(base[u], peak[u])
             factor = jnp.exp2((base[u] - new) * exponent_scale)
             sum_ref[half, h] = (sum_ref[half, h] + part) * factor
             max_ref[half, h, 0:1] = new
 
+        store = project(jnp.minimum(j + 1, 31))
         for u in range(count + 1):
             if u < count:
                 weigh(u)
             if u:
                 gather(u - 1)
+        store()
         most = peak[0] - base[0]
         for u in range(1, count):
             most = jnp.maximum(most, peak[u] - base[u])
         excess_ref[0:1] = jnp.maximum(excess_ref[0:1], most)
 
     def safe_step(j):
-        project(j)
-        for half in range(2):
-            edge = group if half == 0 else 31 - group
-
-            @pl.when(j <= edge)
+        project(j)()
+
+        def one(half, carried):
+            @pl.when(j <= jnp.where(half == 0, group, 31 - group))
             def _():
                 safe_tile(j, half)
+
+            return carried
+
+        lax.fori_loop(0, 2, one, 0)
 
     def one_half(j):
         for half in range(2):
@@ -236,23 +247,16 @@
             def _():
                 tiles(j, (half,), False)
 
-            @pl.when(j == edge)
-            def _():
-                tiles(j, (half,), True)
-
-    clear()
-    excess_ref[...] = jnp.zeros_like(excess_ref)
-    copies[0].wait()
-    lax.fori_loop(0, 1, lambda j, c: (safe_step(j), c)[1], 0)
+        @pl.when(jnp.logical_or(j == group, j == 31 - group))
+        def _():
+            tiles(j, (jnp.where(j == group, 0, 1),), True)
 
     def step(j, carried):
         for n in range(1, chunks):
 
-            @pl.when(j == n * STEPS_A_CHUNK)
+            @pl.when(j + 1 == n * STEPS_A_CHUNK)
             def _():
                 copies[n].wait()
-
-        project(j)
 
         @pl.when(j < low)
         def _():
@@ -264,19 +268,32 @@
 
         return carried
 
-    lax.fori_loop(1, last + 1, step, 0)
+    def attempt(again, carried):
+        worst = jnp.max(excess_ref[0:1]) * exponent_scale
+        redo = jnp.logical_and(again == 1, jnp.logical_not(worst < excess_limit))
+
+        @pl.when(jnp.logical_or(again == 0, redo))
+        def _():
+            clear()
+
+        safe_steps = jnp.where(again == 0, 1, jnp.where(redo, last + 1, 0))
+        lax.fori_loop(0, safe_steps, lambda j, c: (safe_step(j), c)[1], 0)
+
+        @pl.when(again == 0)
+        def _():
+            project(1)()
+
+        lax.fori_loop(1, jnp.where(again == 0, last + 1, 1), step, 0)
+        return carried
+
+    excess_ref[...] = jnp.zeros_like(excess_ref)
+    copies[0].wait()
+    lax.fori_loop(0, 2, attempt, 0)
     for n in range(1, chunks):
 
-        @pl.when(last < n * STEPS_A_CHUNK)
+        @pl.when(last + 1 < n * STEPS_A_CHUNK)
         def _():
             copies[n].wait()
-
-    worst = jnp.max(excess_ref[0:1]) * exponent_scale
-
-    @pl.when(jnp.logical_not(worst < excess_limit))
-    def _():
-        clear()
-        lax.fori_loop(0, last + 1, lambda j, c: (safe_step(j), c)[1], 0)
 
     for half in range(2):
         heads = [
@@ -303,8 +320,8 @@
         scratch_shapes=[
             pltpu.VMEM((128, 288, 128), jnp.bfloat16),
             pltpu.VMEM((2, HEADS_HERE, 256, QUERIES), jnp.bfloat16),
-            pltpu.VMEM((2, KEYS, 256), jnp.bfloat16),
-            pltpu.VMEM((HEADS_HERE, 80, KEYS), jnp.bfloat16),
+            pltpu.VMEM((2, 2, KEYS, 256), jnp.bfloat16),
+            pltpu.VMEM((2, HEADS_HERE, 80, KEYS), jnp.bfloat16),
             pltpu.VMEM((2, HEADS_HERE, 8, QUERIES), jnp.float32),
             pltpu.VMEM((2, HEADS_HERE, 80, QUERIES), jnp.float32),
             pltpu.VMEM((8, QUERIES), jnp.float32),
@@ -318,7 +335,7 @@
     )(place, kv, q, wq_t, wr_t, cosine, sine, wk, wv_t, wo, after)
 
 
-ROWS = 256
+ROWS = 768
 COLUMNS = 512
 IN_FLIGHT = 4
 
@@ -511,15 +528,20 @@
     q_sine = q_sine.reshape(2, QUERIES, ROPE // 2).transpose(0, 2, 1)
 
     gate, up, down = w_gate_exp[0], w_up_exp[0], w_down_exp[0]
+    half_units = down.shape[0] // 2
     gate_left = lax.ppermute(gate, both, shift(1))
     gate_right = lax.ppermute(gate, both, shift(-1))
     up_left = lax.ppermute(up, both, shift(1))
     up_right = lax.ppermute(up, both, shift(-1))
-    down_left = lax.ppermute(down, both, shift(1))
-    down_right = lax.ppermute(down, both, shift(-1))
-    down_across = lax.ppermute(down, both, shift(2))
+    down_top, down_low = down[:half_units], down[half_units:]
+    top_left = lax.ppermute(down_top, both, shift(1))
+    low_right = lax.ppermute(down_low, both, shift(-1))
+    low_left = lax.ppermute(down_low, both, shift(1))
+    top_right = lax.ppermute(down_top, both, shift(-1))
+    top_across = lax.ppermute(top_left, both, shift(1))
+    low_across = lax.ppermute(low_right, both, shift(-1))
     gate_across = lax.ppermute(gate_left, both, shift(1))
-    up_across = lax.ppermute(up_left, both, shift(1))
+    up_across = lax.ppermute(up_right, both, shift(-1))
 
     expert_count = ep_count
     slot_count = 3 * tok_rows * TOPK // (2 * expert_count)
@@ -583,9 +605,9 @@
         chosen,
         [
             ([gate], [up], [down]),
-            ([gate_left], [up_left], [down_left]),
-            ([gate_right], [up_right], [down_right]),
-            ([gate_across], [up_across], [down_across]),
+            ([gate_left], [up_left], [top_left, low_left]),
+            ([gate_right], [up_right], [top_right, low_right]),
+            ([gate_across], [up_across], [top_across, low_across]),
         ],
         None,
         partial_out,

time: 321 us -> 329 us (1.025)
  starting transfers between devices: 40.6 us -> 45.1 us
  waiting for transfers between devices: 94.9 us -> 99.4 us
    ppermute x4 -> x7, waiting for transfers between devices: 0.01 us -> 18.6 us  [the longest x1 9.76 us: layer(): top_across = lax.ppermute(top_left, both, shift(1))]
    ppermute x1, waiting for transfers between devices: 46.1 us -> 32 us  [layer(): q_mirrored = lax.ppermute(q_near[:, tok_rows * 2:], both, mirror)]
    ppermute x4 -> x7, starting transfers between devices: 3.86 us -> 7.1 us  [the longest x1 2.35 us: layer(): low_right = lax.ppermute(down_low, both, shift(-1))]
  transfers between devices with their start and end apart: 21 -> 24, of which waited for: 5 -> 7; matrix products, arithmetic and copies ran while one was open for 8% -> 9% of each run, Pallas kernels for 43% -> 40%
where the time goes in v3:
time: 329 us; the launch traced here: 328 us
  Pallas kernels  133 us (40%)
  waiting for transfers between devices  99.4 us (30%)
  starting transfers between devices  45.1 us (14%)
  other arithmetic  17.7 us (5%)
  between operations  14.5 us (4%)
  local copies, waits for them, and re-layouts  13.3 us (4%)
  matrix products  5.22 us (2%)
    pallas_call x1, Pallas kernels, attention(): pl.pallas_call(attention_kernel, in_specs=[pl.BlockSpec(memory_space=pltp...  110 us
    all_to_all x1, waiting for transfers between devices, layer(): lax.all_to_all(results.reshape(expert_count, slot_count, D), 'ep', split_...  39.6 us
    ppermute x1, waiting for transfers between devices, layer(): q_mirrored = lax.ppermute(q_near[:, tok_rows * 2:], both, mirror)  32 us
    pallas_call x1, Pallas kernels, experts(): pl.pallas_call(body, grid=(rows.shape[0] // ROWS,), in_specs=in_specs, ou...  22.6 us
    all_to_all x1, starting transfers between devices, layer(): lax.all_to_all(outgoing.reshape(expert_count, slot_count, D), 'ep', split...  11.3 us
    ppermute x1, waiting for transfers between devices, layer(): top_across = lax.ppermute(top_left, both, shift(1))  9.76 us
    ppermute x1, waiting for transfers between devices, layer(): low_left = lax.ppermute(down_low, both, shift(1))  8.85 us
    unnamed x37, local copies, waits for them, and re-layouts  7.11 us
  transfers between devices with their start and end apart: 24, of which 7 were waited for; matrix products, arithmetic and copies ran while one was open for 9% of the time, Pallas kernels for 40%

profile of v3, /device:TPU:1, one launch (start us, length us, event | category | flops | bytes accessed | tf_op | source)
XLA Modules:
  0.0 327.8 jit_solution(14261120775697779030)
XLA Ops:
  7.3 0.8 convert_element_type.73
  8.6 1.0 fusion.30
  9.6 0.9 fusion.32
  10.6 2.1 collective-permute-start
  12.7 1.3 collective-permute-start.1
  14.0 1.6 collective-permute-start.2
  15.9 2.9 collective-permute-done.2
  18.8 0.7 pad_maximum_fusion.3
  19.6 1.0 fusion.16
  20.6 1.0 fusion.18
  22.4 2.1 collective-permute-start.4
  24.9 0.8 copy.60
  25.9 1.2 reduce-window.6
  27.9 2.9 convolution_convert_fusion
  30.8 11.3 %all-to-all-start = ((bf16[32,24,2048]{2,1,0:T(8,128)(2,1)}), bf16[32,24,2048]{2,1,0:T(8,128)(2,1)S(1)}, u32[]{:S(2)}, u32[]{:S(2)}) async-start(bf16[32,24,2048]{2,1,0:T(8,128)(2,1)} %bitcast.25), calls=%async_computation.1 | async-start | bytes 6291456 | tf_op jit(solution)/shard_map/all_to_all | solution.py:577
  42.2 2.4 slice_bitcast_fusion
  44.9 2.4 collective-permute-start.15
  47.2 2.7 collective-permute-start.13
  49.9 1.0 pad_maximum_fusion
  51.0 0.7 slice_bitcast_fusion.2
  51.7 6.1 %collective-permute-start.6 = (bf16[4,256,128]{2,1,0:T(8,128)(2,1)}, bf16[4,256,128]{2,1,0:T(8,128)(2,1)}, u32[]{:S(2)}, u32[]{:S(2)}) collective-permute-start(bf16[4,256,128]{2,1,0:T(8,128)(2,1)} %get-tuple-element.7), channel_id=1, source_target_pairs={{0,124},{1,125},{2,126},{3,127},{4,120},{5,121},{6,122},{7,123},{8... | collective-permute-start | bytes 786440 | tf_op jit(solution)/shard_map/ppermute | solution.py:517
  59.0 0.7 add.149
  59.6 0.7 add.153
  60.3 0.7 fusion.47
  61.0 1.8 copy.57
  62.8 0.8 copy.58
  63.6 1.7 copy.59
  65.2 32.0 %collective-permute-done.6 = bf16[4,256,128]{2,1,0:T(8,128)(2,1)} collective-permute-done((bf16[4,256,128]{2,1,0:T(8,128)(2,1)}, bf16[4,256,128]{2,1,0:T(8,128)(2,1)}, u32[]{:S(2)}, u32[]{:S(2)}) %collective-permute-start.6) | collective-permute-done | bytes 262176 | tf_op jit(solution)/shard_map/ppermute | solution.py:517
  97.2 0.7 collective-permute-start.11
  98.0 2.0 collective-permute-start.14
  99.9 1.5 multiply_sine_fusion
  102.1 1.8 pad_maximum_fusion.1.q_ref
  103.8 8.9 %collective-permute-done.11.refs_7_ = bf16[128,2048]{1,0:T(8,128)(2,1)} collective-permute-done((bf16[128,2048]{1,0:T(8,128)(2,1)}, bf16[128,2048]{1,0:T(8,128)(2,1)}, u32[]{:S(2)}, u32[]{:S(2)}) %collective-permute-start.11) | collective-permute-done | bytes 524320 | tf_op jit(solution)/shard_map/ppermute | solution.py:539
  113.0 1.2 collective-permute-start.9
  114.2 9.8 %collective-permute-done.18.refs_14_ = bf16[128,2048]{1,0:T(8,128)(2,1)} collective-permute-done((bf16[128,2048]{1,0:T(8,128)(2,1)}, bf16[128,2048]{1,0:T(8,128)(2,1)}, u32[]{:S(2)}, u32[]{:S(2)}) %collective-permute-start.18) | collective-permute-done | bytes 524320 | tf_op jit(solution)/shard_map/ppermute | solution.py:541
  124.2 1.2 collective-permute-start.16
  125.4 1.5 collective-permute-start.17
  126.9 110.1 %attention.1 = bf16[4,2,64,2048]{3,2,1,0:T(8,128)(2,1)} custom-call(s32[6]{0:T(128)} %pad_add_fusion.place_ref.after_ref, bf16[128,288,128]{2,1,0:T(8,128)(2,1)} %all-gather.2.cloned.1.call-done.kv_ref, bf16[2,4,256,128]{3,2,1,0:T(8,128)(2,1)} %pad_maximum_fusion.1.q_ref, bf16[256,512]{1,0:T(8,128)(2,1)} %bitcast.67, bf16[128,512]{1,0:T(8,128)(2,1)} %bitcast.69, ...), custom_call_target="tpu_custom_call" | custom-call | flops 30000001024 | bytes 16000000 | tf_op jit(solution)/shard_map/attention/pallas_call | solution.py:311
  237.1 1.7 copy-done
  238.8 22.6 %shard_map.176 = bf16[768,2048]{1,0:T(8,128)(2,1)} custom-call(bf16[768,2048]{1,0:T(8,128)(2,1)} %bitcast.62, bf16[2048,256]{1,0:T(8,128)(2,1)} %bitcast.77, bf16[2048,256]{1,0:T(8,128)(2,1)} %bitcast.80, bf16[256,2048]{1,0:T(8,128)(2,1)} %bitcast.66, bf16[2048,256]{1,0:T(8,128)(2,1)} %collective-permute-done.8.refs_4_, ...), custom_call_target="tpu_custom_call" | custom-call | flops 9663676416 | bytes 24000000 | tf_op jit(solution)/shard_map/pallas_call | solution.py:427
  261.4 5.0 %all-to-all-start.1 = ((bf16[32,24,2048]{2,1,0:T(8,128)(2,1)}), bf16[32,24,2048]{2,1,0:T(8,128)(2,1)S(1)}, u32[]{:S(2)}, u32[]{:S(2)}) async-start(bf16[32,24,2048]{2,1,0:T(8,128)(2,1)} %bitcast.63), calls=%async_computation.2 | async-start | bytes 6291456 | tf_op jit(solution)/shard_map/all_to_all | solution.py:616
  266.7 39.6 %all-to-all-done.1 = bf16[32,24,2048]{2,1,0:T(8,128)(2,1)S(1)} async-done(((bf16[32,24,2048]{2,1,0:T(8,128)(2,1)}), bf16[32,24,2048]{2,1,0:T(8,128)(2,1)S(1)}, u32[]{:S(2)}, u32[]{:S(2)}) %all-to-all-start.1) | async-done | bytes 3145760 | tf_op jit(solution)/shard_map/all_to_all | solution.py:616
  306.3 2.3 fusion.7
  308.6 1.1 fusion.52
  309.7 1.9 collective-permute-start.7
  311.6 2.5 fusion.3
  314.0 6.1 %collective-permute-done.7 = bf16[64,2048]{1,0:T(8,128)(2,1)S(1)} collective-permute-done((bf16[64,2048]{1,0:T(8,128)(2,1)S(1)}, bf16[64,2048]{1,0:T(8,128)(2,1)S(1)}, u32[]{:S(2)}, u32[]{:S(2)}) %collective-permute-start.7) | collective-permute-done | bytes 262176 | tf_op jit(solution)/shard_map/ppermute | solution.py:601
  320.2 0.8 pad_maximum_fusion.2
  (91 shorter events, 6.0 us)
Async XLA Ops:
  7.2 20.7 %copy-start.4 = (s32[128,4]{0,1:T(4,128)S(1)}, s32[128,4]{0,1:T(4,128)}, u32[]{:S(2)}) copy-start(s32[128,4]{0,1:T(4,128)} %param.29) | copy-start | bytes 6148
  7.2 20.4 %copy-start.1 = (bf16[128,2048]{1,0:T(8,128)(2,1)S(1)}, bf16[128,2048]{1,0:T(8,128)(2,1)}, u32[]{:S(2)}) copy-start(bf16[128,2048]{1,0:T(8,128)(2,1)} %param.27) | copy-start | bytes 1572868
  7.2 20.7 %copy-start.3 = (f32[2048]{0:T(1024)S(1)}, f32[2048]{0:T(1024)}, u32[]{:S(2)}) copy-start(f32[2048]{0:T(1024)} %param.28) | copy-start | bytes 24580
  7.2 119.7 %all-gather.2.cloned.1.call-start = ((), (), s32[]{:S(2)}) async-start(), calls=%async_computation.3 | async-start | bytes 9732096 | tf_op jit(solution)/shard_map/all_gather | solution.py:510
  7.3 0.9 copy-start.9
  10.6 5.2 %collective-permute-start = (bf16[288,128]{1,0:T(8,128)(2,1)S(1)}, bf16[288,128]{1,0:T(8,128)(2,1)S(1)}, u32[]{:S(2)}, u32[]{:S(2)}) collective-permute-start(bf16[288,128]{1,0:T(8,128)(2,1)S(1)} %maximum_maximum_fusion), channel_id=1, source_target_pairs={{0,1},{1,2},{2,3},{3,0},{4,5},{5,6},{6,7},{7,4},{8,9},{9,10},{10,1... | collective-permute-start | bytes 221192 | tf_op jit(solution)/shard_map/ppermute | solution.py:502
  12.7 3.2 collective-permute-start.1
  14.0 4.8 %collective-permute-start.2 = (bf16[288,128]{1,0:T(8,128)(2,1)S(1)}, bf16[288,128]{1,0:T(8,128)(2,1)S(1)}, u32[]{:S(2)}, u32[]{:S(2)}) collective-permute-start(bf16[288,128]{1,0:T(8,128)(2,1)S(1)} %maximum_maximum_fusion), channel_id=1, source_target_pairs={{0,2},{1,3},{2,0},{3,1},{4,6},{5,7},{6,4},{7,5},{8,10},{9,11},{10,... | collective-permute-start | bytes 221192 | tf_op jit(solution)/shard_map/ppermute | solution.py:504
  21.7 25.5 %collective-permute-start.3 = (bf16[512,128]{1,0:T(8,128)(2,1)S(1)}, bf16[512,128]{1,0:T(8,128)(2,1)S(1)}, u32[]{:S(2)}, u32[]{:S(2)}) collective-permute-start(bf16[512,128]{1,0:T(8,128)(2,1)S(1)} %constant_dynamic-update-slice_fusion), channel_id=1, source_target_pairs={{0,1},{1,2},{2,3},{3,0},{4,5},{5,6},{6,7},{7,4},{8,9},{9,10},{10,1... | collective-permute-start | bytes 393224 | tf_op jit(solution)/shard_map/ppermute | solution.py:502
  22.4 24.9 %collective-permute-start.4 = (bf16[512,128]{1,0:T(8,128)(2,1)S(1)}, bf16[512,128]{1,0:T(8,128)(2,1)}, u32[]{:S(2)}, u32[]{:S(2)}) collective-permute-start(bf16[512,128]{1,0:T(8,128)(2,1)S(1)} %constant_dynamic-update-slice_fusion), channel_id=1, source_target_pairs={{0,3},{1,0},{2,1},{3,2},{4,7},{5,4},{6,5},{7,6},{8,11},{9,8},{10,9... | collective-permute-start | bytes 393224 | tf_op jit(solution)/shard_map/ppermute | solution.py:503
  24.5 25.4 %collective-permute-start.5 = (bf16[512,128]{1,0:T(8,128)(2,1)S(1)}, bf16[512,128]{1,0:T(8,128)(2,1)}, u32[]{:S(2)}, u32[]{:S(2)}) collective-permute-start(bf16[512,128]{1,0:T(8,128)(2,1)S(1)} %constant_dynamic-update-slice_fusion), channel_id=1, source_target_pairs={{0,2},{1,3},{2,0},{3,1},{4,6},{5,7},{6,4},{7,5},{8,10},{9,11},{10,... | collective-permute-start | bytes 393224 | tf_op jit(solution)/shard_map/ppermute | solution.py:504
  27.9 2.9 copy-start.5
  27.9 2.9 copy-start.7
  30.8 206.3 %all-to-all-start = ((bf16[32,24,2048]{2,1,0:T(8,128)(2,1)}), bf16[32,24,2048]{2,1,0:T(8,128)(2,1)S(1)}, u32[]{:S(2)}, u32[]{:S(2)}) async-start(bf16[32,24,2048]{2,1,0:T(8,128)(2,1)} %bitcast.25), calls=%async_computation.1 | async-start | bytes 6291456 | tf_op jit(solution)/shard_map/all_to_all | solution.py:577
  42.1 20.7 %copy-start.2 = (bf16[512,128]{1,0:T(8,128)(2,1)S(1)}, bf16[512,128]{1,0:T(8,128)(2,1)}, u32[]{:S(2)}) copy-start(bf16[512,128]{1,0:T(8,128)(2,1)} %param.23) | copy-start | bytes 393220
  42.1 266.5 %reduce-scatter.2.cloned.1.call-start = ((), (), s32[]{:S(2)}) async-start(), calls=%async_computation.4 | async-start | bytes 2621440 | tf_op jit(solution)/shard_map/reduce_scatter | solution.py:599
  44.6 53.4 %collective-permute-start.10 = (bf16[128,2048]{1,0:T(8,128)(2,1)}, bf16[128,2048]{1,0:T(8,128)(2,1)}, u32[]{:S(2)}, u32[]{:S(2)}) collective-permute-start(bf16[128,2048]{1,0:T(8,128)(2,1)} %get-tuple-element.3), channel_id=1, source_target_pairs={{0,1},{1,2},{2,3},{3,0},{4,5},{5,6},{6,7},{7,4},{8,9},{9,10},{10,1... | collective-permute-start | bytes 1572872 | tf_op jit(solution)/shard_map/ppermute | solution.py:537
  44.9 55.1 %collective-permute-start.15 = (bf16[128,2048]{1,0:T(8,128)(2,1)}, bf16[128,2048]{1,0:T(8,128)(2,1)}, u32[]{:S(2)}, u32[]{:S(2)}) collective-permute-start(bf16[128,2048]{1,0:T(8,128)(2,1)} %get-tuple-element.2), channel_id=1, source_target_pairs={{0,3},{1,0},{2,1},{3,2},{4,7},{5,4},{6,5},{7,6},{8,11},{9,8},{10,9... | collective-permute-start | bytes 1572872 | tf_op jit(solution)/shard_map/ppermute | solution.py:538
  47.2 77.0 %collective-permute-start.8 = (bf16[2048,256]{1,0:T(8,128)(2,1)}, bf16[2048,256]{1,0:T(8,128)(2,1)}, u32[]{:S(2)}, u32[]{:S(2)}) collective-permute-start(bf16[2048,256]{1,0:T(8,128)(2,1)} %bitcast.75), channel_id=1, source_target_pairs={{0,1},{1,2},{2,3},{3,0},{4,5},{5,6},{6,7},{7,4},{8,9},{9,10},{10,1... | collective-permute-start | bytes 3145736 | tf_op jit(solution)/shard_map/ppermute | solution.py:532
  47.2 78.2 %collective-permute-start.13 = (bf16[2048,256]{1,0:T(8,128)(2,1)}, bf16[2048,256]{1,0:T(8,128)(2,1)}, u32[]{:S(2)}, u32[]{:S(2)}) collective-permute-start(bf16[2048,256]{1,0:T(8,128)(2,1)} %bitcast.78), channel_id=1, source_target_pairs={{0,3},{1,0},{2,1},{3,2},{4,7},{5,4},{6,5},{7,6},{8,11},{9,8},{10,9... | collective-permute-start | bytes 3145736 | tf_op jit(solution)/shard_map/ppermute | solution.py:535
  51.7 45.5 %collective-permute-start.6 = (bf16[4,256,128]{2,1,0:T(8,128)(2,1)}, bf16[4,256,128]{2,1,0:T(8,128)(2,1)}, u32[]{:S(2)}, u32[]{:S(2)}) collective-permute-start(bf16[4,256,128]{2,1,0:T(8,128)(2,1)} %get-tuple-element.7), channel_id=1, source_target_pairs={{0,124},{1,125},{2,126},{3,127},{4,120},{5,121},{6,122},{7,123},{8... | collective-permute-start | bytes 786440 | tf_op jit(solution)/shard_map/ppermute | solution.py:517
  97.2 15.5 %collective-permute-start.11 = (bf16[128,2048]{1,0:T(8,128)(2,1)}, bf16[128,2048]{1,0:T(8,128)(2,1)}, u32[]{:S(2)}, u32[]{:S(2)}) collective-permute-start(bf16[128,2048]{1,0:T(8,128)(2,1)} %get-tuple-element.2), channel_id=1, source_target_pairs={{0,1},{1,2},{2,3},{3,0},{4,5},{5,6},{6,7},{7,4},{8,9},{9,10},{10,1... | collective-permute-start | bytes 1572872 | tf_op jit(solution)/shard_map/ppermute | solution.py:539
  98.0 15.0 %collective-permute-start.14 = (bf16[128,2048]{1,0:T(8,128)(2,1)}, bf16[128,2048]{1,0:T(8,128)(2,1)}, u32[]{:S(2)}, u32[]{:S(2)}) collective-permute-start(bf16[128,2048]{1,0:T(8,128)(2,1)} %get-tuple-element.3), channel_id=1, source_target_pairs={{0,3},{1,0},{2,1},{3,2},{4,7},{5,4},{6,5},{7,6},{8,11},{9,8},{10,9... | collective-permute-start | bytes 1572872 | tf_op jit(solution)/shard_map/ppermute | solution.py:540
  99.9 24.0 %collective-permute-start.18 = (bf16[128,2048]{1,0:T(8,128)(2,1)}, bf16[128,2048]{1,0:T(8,128)(2,1)}, u32[]{:S(2)}, u32[]{:S(2)}) collective-permute-start(bf16[128,2048]{1,0:T(8,128)(2,1)} %collective-permute-done.10.refs_6_), channel_id=1, source_target_pairs={{0,1},{1,2},{2,3},{3,0},{4,5},{5,6},{6,7},{7,4},{8,9},{9,10},{10,1... | collective-permute-start | bytes 1572872 | tf_op jit(solution)/shard_map/ppermute | solution.py:541
  112.7 124.4 %collective-permute-start.12 = (bf16[2048,256]{1,0:T(8,128)(2,1)}, bf16[2048,256]{1,0:T(8,128)(2,1)}, u32[]{:S(2)}, u32[]{:S(2)}) collective-permute-start(bf16[2048,256]{1,0:T(8,128)(2,1)} %bitcast.76), channel_id=1, source_target_pairs={{0,3},{1,0},{2,1},{3,2},{4,7},{5,4},{6,5},{7,6},{8,11},{9,8},{10,9... | collective-permute-start | bytes 3145736 | tf_op jit(solution)/shard_map/ppermute | solution.py:533
  113.0 124.1 %collective-permute-start.9 = (bf16[2048,256]{1,0:T(8,128)(2,1)}, bf16[2048,256]{1,0:T(8,128)(2,1)}, u32[]{:S(2)}, u32[]{:S(2)}) collective-permute-start(bf16[2048,256]{1,0:T(8,128)(2,1)} %bitcast.79), channel_id=1, source_target_pairs={{0,1},{1,2},{2,3},{3,0},{4,5},{5,6},{6,7},{7,4},{8,9},{9,10},{10,1... | collective-permute-start | bytes 3145736 | tf_op jit(solution)/shard_map/ppermute | solution.py:534
  123.9 113.1 %collective-permute-start.19 = (bf16[128,2048]{1,0:T(8,128)(2,1)}, bf16[128,2048]{1,0:T(8,128)(2,1)}, u32[]{:S(2)}, u32[]{:S(2)}) collective-permute-start(bf16[128,2048]{1,0:T(8,128)(2,1)} %collective-permute-done.15.refs_11_), channel_id=1, source_target_pairs={{0,3},{1,0},{2,1},{3,2},{4,7},{5,4},{6,5},{7,6},{8,11},{9,8},{10,9... | collective-permute-start | bytes 1572872 | tf_op jit(solution)/shard_map/ppermute | solution.py:542
  124.2 112.9 %collective-permute-start.16 = (bf16[2048,256]{1,0:T(8,128)(2,1)}, bf16[2048,256]{1,0:T(8,128)(2,1)}, u32[]{:S(2)}, u32[]{:S(2)}) collective-permute-start(bf16[2048,256]{1,0:T(8,128)(2,1)} %collective-permute-done.8.refs_4_), channel_id=1, source_target_pairs={{0,1},{1,2},{2,3},{3,0},{4,5},{5,6},{6,7},{7,4},{8,9},{9,10},{10,1... | collective-permute-start | bytes 3145736 | tf_op jit(solution)/shard_map/ppermute | solution.py:543
  125.4 111.7 %collective-permute-start.17 = (bf16[2048,256]{1,0:T(8,128)(2,1)}, bf16[2048,256]{1,0:T(8,128)(2,1)}, u32[]{:S(2)}, u32[]{:S(2)}) collective-permute-start(bf16[2048,256]{1,0:T(8,128)(2,1)} %collective-permute-done.13.refs_9_), channel_id=1, source_target_pairs={{0,3},{1,0},{2,1},{3,2},{4,7},{5,4},{6,5},{7,6},{8,11},{9,8},{10,9... | collective-permute-start | bytes 3145736 | tf_op jit(solution)/shard_map/ppermute | solution.py:544
  237.1 1.7 copy-start
  261.4 5.0 %copy-start.10 = (f32[128,4]{0,1:T(4,128)S(1)}, f32[128,4]{0,1:T(4,128)}, u32[]{:S(2)}) copy-start(f32[128,4]{0,1:T(4,128)} %param.30) | copy-start | bytes 6148
  261.4 5.0 %copy-start.6 = (s32[128]{0:T(128)S(1)}, s32[128]{0:T(128)}, u32[]{:S(2)}) copy-start(s32[128]{0:T(128)} %copy-done.5) | copy-start | bytes 1540
  261.4 5.0 %copy-start.8 = (s32[128]{0:T(128)S(1)}, s32[128]{0:T(128)}, u32[]{:S(2)}) copy-start(s32[128]{0:T(128)} %copy-done.7) | copy-start | bytes 1540
  261.4 44.9 %all-to-all-start.1 = ((bf16[32,24,2048]{2,1,0:T(8,128)(2,1)}), bf16[32,24,2048]{2,1,0:T(8,128)(2,1)S(1)}, u32[]{:S(2)}, u32[]{:S(2)}) async-start(bf16[32,24,2048]{2,1,0:T(8,128)(2,1)} %bitcast.63), calls=%async_computation.2 | async-start | bytes 6291456 | tf_op jit(solution)/shard_map/all_to_all | solution.py:616
  309.7 10.5 %collective-permute-start.7 = (bf16[64,2048]{1,0:T(8,128)(2,1)S(1)}, bf16[64,2048]{1,0:T(8,128)(2,1)S(1)}, u32[]{:S(2)}, u32[]{:S(2)}) collective-permute-start(bf16[64,2048]{1,0:T(8,128)(2,1)S(1)} %get-tuple-element.5), channel_id=1, source_target_pairs={{0,124},{1,125},{2,126},{3,127},{4,120},{5,121},{6,122},{7,123},{8... | collective-permute-start | bytes 786440 | tf_op jit(solution)/shard_map/ppermute | solution.py:601
Sparse Core Ops, SparseCore 0:
  19.7 87.3 all-gather.1
  237.2 25.7 reduce-scatter.1
